TPU v7x, 32 devices: a whole 2x2x4 slice. The times are simulated.
32 devices in a mesh: sp: 8 (over z, x), tp: 4 (over y, core).
Axes of the slice: x: 2, y: 2, z: 4, core: 2. Of those that a mesh axis runs over, the one named last changes fastest.
Arguments:
- pool_in: bfloat16 [2048, 512], P('sp', 'tp'), may hold values from -6 to 6
- pool_weight: bfloat16 [4, 128, 128], P('tp'), may hold values from -0.5 to 0.5
- pool_scale: float32 [512], P('tp'), may hold values from 0.1 to 1.9
- pool_norm: float32 [512], replicated, may hold values from 0.1 to 1.9
- out_weight: bfloat16 [512, 2048], replicated, may hold values from -0.25 to 0.25
- stream: bfloat16 [2048, 2048], P('sp'), may hold values from -6 to 6
- mix_norm: float32 [2048], replicated, may hold values from 0.1 to 1.9
- ffn_norm: float32 [2048], replicated, may hold values from 0.1 to 1.9
- routes: int32 [2048, 4], P('sp'), may hold values from 0 to 7, all different within a row; in each aligned block of 256 rows (0 to 255, 256 to 511, ...) at most 192 rows name the same one
- route_weights: float32 [2048, 4], P('sp'), may hold values from 0.1 to 1
- w_gate: bfloat16 [8, 2048, 2048], P('sp', None, 'tp'), may hold values from -0.125 to 0.125
- w_up: bfloat16 [8, 2048, 2048], P('sp', None, 'tp'), may hold values from -0.125 to 0.125
- gate_bias: float32 [8, 2048], P('sp', 'tp'), may hold values from -12 to 12
- up_bias: float32 [8, 2048], P('sp', 'tp'), may hold values from -12 to 12
- w_down: bfloat16 [8, 2048, 2048], P('sp', 'tp'), may hold values from -2 to 2
- expert_norm: float32 [2048], P('tp'), may hold values from 0.1 to 1.9
Outputs:
- result: bfloat16 [2048, 2048], P('sp', 'tp')
Inputs may be any that keep to these rules, and one draw needn't show every extreme that they name: `routes`: each row names 4 different experts. In each aligned block of 256 tokens no expert is named by more than 192 tokens, a bound that some block reaches.
All inputs are finite; a program needn't handle non-finite values.
Results may differ from a plain program's by a relative error of at most 0.012.
Values may be sent and summed in bfloat16 or wider, within the bound.
A program may use at most 128 MiB of HBM per device.

v0:
```python
import jax
import jax.numpy as jnp
from jax import lax
from jax.sharding import PartitionSpec as P

epsilon = 1e-06
reach_rows = 8
clamp_limit = 7.0
sigmoid_alpha = 1.702
chunk_counts = (2,)


def extended_2(shard, sides, width):
    for axis, dim in sides:
        count, length = (lax.axis_size(axis), shard.shape[dim])
        up = [(i, (i + 1) % count) for i in range(count - 1)]
        down = [(j, i) for i, j in up]
        last = lax.slice_in_dim(shard, length - width, length, axis=dim)
        leading = lax.slice_in_dim(shard, 0, width, axis=dim)
        before = lax.ppermute(last, axis, up)
        after = lax.ppermute(leading, axis, down)
        shard = jnp.concatenate([before, shard, after], axis=dim)
    return shard


def rms_scale(values):
    return values * lax.rsqrt(jnp.mean(values * values, axis=-1, keepdims=True) + epsilon)


def shards(
    pool_in,
    pool_weight,
    pool_scale,
    pool_norm,
    out_weight,
    stream,
    mix_norm,
    ffn_norm,
    routes,
    route_weights,
    w_gate,
    w_up,
    gate_bias,
    up_bias,
    w_down,
    expert_norm,
):
    rows_dev = pool_in.shape[0]
    length = rows_dev * lax.axis_size("sp")
    radius = jnp.left_shift(1, lax.axis_index("tp"))
    positions = lax.axis_index("sp") * rows_dev + jnp.arange(rows_dev)
    padded = extended_2(pool_in, (("sp", 0),), reach_rows).astype(jnp.float32)
    window_sum = jnp.zeros((rows_dev, pool_in.shape[1]), jnp.float32)
    counts = jnp.zeros((rows_dev,), jnp.float32)
    for offset in range(-reach_rows, reach_rows + 1):
        inside = (positions + offset >= 0) & (positions + offset < length) & (abs(offset) <= radius)
        window_sum = window_sum + jnp.where(
            inside[:, None], padded[reach_rows + offset : reach_rows + offset + rows_dev], 0.0
        )
        counts = counts + inside.astype(jnp.float32)
    deviation = (window_sum / counts[:, None] - padded[reach_rows : reach_rows + rows_dev]).astype(
        jnp.bfloat16
    )
    pool_out = (
        jnp.dot(deviation, pool_weight[0], preferred_element_type=jnp.float32) * pool_scale
    ).astype(jnp.bfloat16)
    all_groups = lax.all_gather(pool_out, "tp", axis=1, tiled=True)
    normed = (rms_scale(all_groups.astype(jnp.float32)) * pool_norm).astype(jnp.bfloat16)
    mix_out = jnp.dot(normed, out_weight, preferred_element_type=jnp.float32)
    mixed = (stream.astype(jnp.float32) + rms_scale(mix_out) * mix_norm).astype(jnp.bfloat16)
    expert_in = (rms_scale(mixed.astype(jnp.float32)) * ffn_norm).astype(jnp.bfloat16)
    model_width = mixed.shape[1]
    experts = lax.axis_size("sp") * w_gate.shape[0]
    top_count = routes.shape[1]
    capacity = rows_dev * top_count * 3 // (2 * experts)
    quarter = capacity // lax.axis_size("tp")
    chunks = next((n for n in chunk_counts if quarter % (8 * n) == 0), 1)
    chunk_rows, own_rows = capacity // chunks, quarter // chunks

    names = routes.T[:, None, :] == jnp.arange(experts, dtype=jnp.int32)[None, :, None]
    member = jnp.any(names, axis=0)
    weight = jnp.sum(jnp.where(names, route_weights.T[:, None, :], 0.0), axis=0)
    order = jnp.arange(rows_dev)
    earlier = (order[:, None] < order[None, :]).astype(jnp.bfloat16)
    place = jnp.dot(
        member.astype(jnp.bfloat16), earlier, preferred_element_type=jnp.float32
    ).astype(jnp.int32)
    place = jnp.where(member, place, -1)

    def dispatched(chunk):
        first = chunk * chunk_rows + lax.axis_index("tp") * own_rows
        slots = first + jnp.arange(own_rows, dtype=jnp.int32)
        pick = (place[:, None, :] == slots[None, :, None]).astype(jnp.bfloat16)
        rows = jnp.dot(pick.reshape(experts * own_rows, rows_dev), expert_in)
        own_slots = rows.reshape(experts, own_rows, model_width)
        arrived = lax.all_to_all(own_slots, "sp", split_axis=0, concat_axis=0, tiled=True)
        return lax.all_gather(arrived, "tp", axis=1, tiled=True)

    def expert(slot_block):
        row_block = slot_block.reshape(-1, model_width)
        gate_pre = jnp.dot(row_block, w_gate[0], preferred_element_type=jnp.float32) + gate_bias[0]
        up_pre = jnp.dot(row_block, w_up[0], preferred_element_type=jnp.float32) + up_bias[0]
        gate_cut = jnp.minimum(gate_pre, clamp_limit)
        up_cut = jnp.clip(up_pre, -clamp_limit, clamp_limit)
        activation = (
            (up_cut + 1.0) * (gate_cut * jax.nn.sigmoid(sigmoid_alpha * gate_cut))
        ).astype(jnp.bfloat16)
        partial_value = jnp.dot(activation, w_down[0], preferred_element_type=jnp.float32).astype(
            jnp.bfloat16
        )
        partial_value = partial_value.reshape(slot_block.shape)
        summed = lax.psum_scatter(partial_value, "tp", scatter_dimension=2, tiled=True)
        return lax.all_to_all(summed, "sp", split_axis=0, concat_axis=0, tiled=True)

    def weighted(chunk, returned):
        slots = chunk * chunk_rows + jnp.arange(chunk_rows, dtype=jnp.int32)
        spread = jnp.where(place[:, None, :] == slots[None, :, None], weight[:, None, :], 0.0)
        spread = spread.reshape(experts * chunk_rows, rows_dev)
        high = spread.astype(jnp.bfloat16)
        low = (spread - high.astype(jnp.float32)).astype(jnp.bfloat16)
        flat = returned.reshape(experts * chunk_rows, -1)
        over_slots = (((0,), (0,)), ((), ()))
        return lax.dot_general(
            high, flat, over_slots, preferred_element_type=jnp.float32
        ) + lax.dot_general(low, flat, over_slots, preferred_element_type=jnp.float32)

    blocks = [dispatched(chunk) for chunk in range(chunks)]
    parts = [expert(block) for block in blocks]
    col_count = parts[0].shape[2]
    combined = sum(weighted(chunk, part) for chunk, part in enumerate(parts))
    squares = lax.psum(jnp.sum(combined * combined, axis=1), "tp")
    row_scale = lax.rsqrt(squares / model_width + epsilon)
    own_cols = lax.dynamic_slice_in_dim(
        mixed.astype(jnp.float32), lax.axis_index("tp") * col_count, col_count, 1
    )
    return (own_cols + combined * row_scale[:, None] * expert_norm).astype(jnp.bfloat16)


def solution(mesh):
    in_specs = (
        P("sp", "tp"),
        P("tp", None, None),
        P("tp"),
        P(),
        P(),
        P("sp", None),
        P(),
        P(),
        P("sp", None),
        P("sp", None),
        P("sp", None, "tp"),
        P("sp", None, "tp"),
        P("sp", "tp"),
        P("sp", "tp"),
        P("sp", "tp", None),
        P("tp"),
    )
    out_specs = P("sp", "tp")
    return jax.shard_map(shards, mesh=mesh, in_specs=in_specs, out_specs=out_specs, check_vma=False)
```

profile of v0, /device:TPU:0, one launch (start us, length us, event | category | flops | bytes accessed | tf_op | source)
XLA Modules:
  0.0 238.6 jit_solution(14697897174316907581)
XLA Ops:
  7.4 1.3 collective-permute-start.1
  8.7 5.5 %collective-permute-start = (bf16[8,128]{1,0:T(8,128)(2,1)S(1)}, bf16[8,128]{1,0:T(8,128)(2,1)S(1)}, u32[]{:S(2)}, u32[]{:S(2)}) collective-permute-start(bf16[8,128]{1,0:T(8,128)(2,1)S(1)} %get-tuple-element.25), channel_id=1, source_target_pairs={{0,4},{4,8},{8,12},{12,16},{16,20},{20,24},{24,28},{1,5},{5,9},{9,... | collective-permute-start | bytes 6152 | tf_op jit(solution)/shard_map/ppermute | solution.py:20
  16.4 2.6 %fusion.17 = bf16[256,128]{1,0:T(8,128)(2,1)S(1)} fusion(f32[128]{0:T(128)} %param.18, f32[272,128]{1,0:T(8,128)S(1)} %maximum_convert_fusion, f32[256]{0:T(256)S(1)} %get-tuple-element.7, pred[256]{0:T(512)(128)(4,1)S(1)} %get-tuple-element.24, pred[256]{0:T(512)(128)(4,1)S(1)} %get-tuple-element.23, pred[256]{0:T(512)(128)(4,1)S(1)} %get-tuple-element.22, ...), kind=kOutput, calls=%fused_computation.26 | convolution fusion | flops 9633792 | bytes 2336768 | tf_op jit(solution)/shard_map/dot_general | solution.py:65
  19.0 6.3 %all_gather.9 = bf16[256,512]{1,0:T(8,128)(2,1)S(1)} all-gather(bf16[256,128]{1,0:T(8,128)(2,1)S(1)} %fusion.17), channel_id=1, replica_groups=mesh['sp'=8,'tp'=4] {'tp'}, dimensions={1}, use_global_device_ids=true | all-gather | bytes 327680 | tf_op jit(solution)/shard_map/all_gather | solution.py:67
  25.5 0.9 multiply_reduce_fusion.1
  27.2 1.3 copy-done.1
  29.0 28.0 %all_to_all.20 = bf16[8,24,2048]{2,1,0:T(8,128)(2,1)} all-to-all(bf16[8,24,2048]{2,1,0:T(8,128)(2,1)S(1)} %fusion.50), channel_id=1, replica_groups=mesh['sp'=8,'tp'=4] {'sp'}, dimensions={0} | all-to-all | bytes 1572864 | tf_op jit(solution)/shard_map/all_to_all | solution.py:96
  57.1 2.1 fusion.52
  59.2 23.8 %all_to_all.21 = bf16[8,24,2048]{2,1,0:T(8,128)(2,1)} all-to-all(bf16[8,24,2048]{2,1,0:T(8,128)(2,1)S(1)} %fusion.52), channel_id=1, replica_groups=mesh['sp'=8,'tp'=4] {'sp'}, dimensions={0} | all-to-all | bytes 1572864 | tf_op jit(solution)/shard_map/all_to_all | solution.py:96
  83.0 1.8 all-gather.5.cloned.1.call-done
  84.8 5.6 %fusion.2 = f32[768,512]{1,0:T(8,128)} fusion(bf16[768,2048]{1,0:T(8,128)(2,1)} %bitcast.69, bf16[1,2048,512]{2,1,0:T(8,128)(2,1)} %param.26), kind=kOutput, calls=%fused_computation.4 | convolution fusion | flops 1610612736 | bytes 6815744 | tf_op jit(solution)/shard_map/dot_general | solution.py:101
  90.3 8.8 %convolution_convert_fusion = bf16[768,2048]{1,0:T(8,128)(2,1)} fusion(bf16[1,512,2048]{2,1,0:T(8,128)(2,1)S(1)} %copy-done, f32[768,512]{1,0:T(8,128)} %fusion.2, bf16[768,2048]{1,0:T(8,128)(2,1)} %bitcast.70, bf16[1,2048,512]{2,1,0:T(8,128)(2,1)} %param.27, f32[512]{0:T(512)S(1)} %bitcast.71, f32[512]{0:T(512)S(1)} %bitcast.73), kind=kOutput, calls=%fused_computation | convolution fusion | flops 3227516928 | bytes 12062720 | tf_op jit(solution)/shard_map/dot_general | solution.py:108
  99.2 15.7 %all-gather.3.cloned.1.call-done = bf16[8,96,2048]{2,1,0:T(8,128)(2,1)} async-done(((bf16[8,24,2048]{2,1,0:T(8,128)(2,1)}), bf16[8,96,2048]{2,1,0:T(8,128)(2,1)}) %all-gather.3.cloned.1.call-update) | async-done | bytes 3145744 | tf_op jit(solution)/shard_map/all_gather | solution.py:97
  114.9 5.5 %fusion.4 = f32[768,512]{1,0:T(8,128)} fusion(bf16[768,2048]{1,0:T(8,128)(2,1)} %bitcast.67, bf16[1,2048,512]{2,1,0:T(8,128)(2,1)} %param.26), kind=kOutput, calls=%fused_computation.6 | convolution fusion | flops 1610612736 | bytes 6815744 | tf_op jit(solution)/shard_map/dot_general | solution.py:101
  120.4 9.0 %convolution_convert_fusion.1 = bf16[768,2048]{1,0:T(8,128)(2,1)} fusion(bf16[1,512,2048]{2,1,0:T(8,128)(2,1)S(1)} %copy-done, f32[768,512]{1,0:T(8,128)} %fusion.4, bf16[768,2048]{1,0:T(8,128)(2,1)} %bitcast.68, bf16[1,2048,512]{2,1,0:T(8,128)(2,1)} %param.27, f32[512]{0:T(512)S(1)} %bitcast.72, f32[512]{0:T(512)S(1)} %bitcast.74), kind=kOutput, calls=%fused_computation.1 | convolution fusion | flops 3227516928 | bytes 12062720 | tf_op jit(solution)/shard_map/dot_general | solution.py:108
  129.4 25.7 %reduce-scatter.5.cloned.1.call-done = bf16[8,96,512]{2,1,0:T(8,128)(2,1)} async-done(((bf16[8,96,2048]{2,1,0:T(8,128)(2,1)}), bf16[8,96,512]{2,1,0:T(8,128)(2,1)}) %reduce-scatter.5.cloned.1.call-update) | async-done | bytes 786448 | tf_op jit(solution)/shard_map/reduce_scatter | solution.py:112
  155.1 5.5 %all-to-all-start.3 = ((bf16[8,96,512]{2,1,0:T(8,128)(2,1)}), bf16[8,96,512]{2,1,0:T(8,128)(2,1)S(1)}, u32[]{:S(2)}, u32[]{:S(2)}) async-start(bf16[8,96,512]{2,1,0:T(8,128)(2,1)} %reduce-scatter.5.cloned.1.call-done), calls=%async_computation.5 | async-start | bytes 1572864 | tf_op jit(solution)/shard_map/all_to_all | solution.py:113
  160.7 34.6 %reduce-scatter.3.cloned.1.call-done = bf16[8,96,512]{2,1,0:T(8,128)(2,1)} async-done(((bf16[8,96,2048]{2,1,0:T(8,128)(2,1)}), bf16[8,96,512]{2,1,0:T(8,128)(2,1)}) %reduce-scatter.3.cloned.1.call-update) | async-done | bytes 786448 | tf_op jit(solution)/shard_map/reduce_scatter | solution.py:112
  195.3 5.5 %all-to-all-start.1 = ((bf16[8,96,512]{2,1,0:T(8,128)(2,1)}), bf16[8,96,512]{2,1,0:T(8,128)(2,1)}, u32[]{:S(2)}, u32[]{:S(2)}) async-start(bf16[8,96,512]{2,1,0:T(8,128)(2,1)} %reduce-scatter.3.cloned.1.call-done), calls=%async_computation.2 | async-start | bytes 1572864 | tf_op jit(solution)/shard_map/all_to_all | solution.py:113
  201.8 19.2 %all-to-all-done.1 = bf16[8,96,512]{2,1,0:T(8,128)(2,1)} async-done(((bf16[8,96,512]{2,1,0:T(8,128)(2,1)}), bf16[8,96,512]{2,1,0:T(8,128)(2,1)}, u32[]{:S(2)}, u32[]{:S(2)}) %all-to-all-start.1) | async-done | bytes 786464 | tf_op jit(solution)/shard_map/all_to_all | solution.py:113
  221.0 1.5 convolution_bitcast_fusion.2
  222.5 1.7 multiply_reduce_fusion.2
  224.2 6.0 %psum.7 = f32[256]{0:T(256)S(1)} all-reduce(f32[256]{0:T(256)S(1)} %get-tuple-element.29), channel_id=1, replica_groups=mesh['sp'=8,'tp'=4] {'tp'}, use_global_device_ids=true, to_apply=%region_8.9 | all-reduce | flops 256 | bytes 2048 | tf_op jit(solution)/shard_map/psum | solution.py:131
  230.1 1.9 add_convert_fusion.1
  (52 shorter events, 5.7 us)
Async XLA Ops:
  6.5 83.8 %copy-start = (bf16[1,512,2048]{2,1,0:T(8,128)(2,1)S(1)}, bf16[1,512,2048]{2,1,0:T(8,128)(2,1)}, u32[]{:S(2)}) copy-start(bf16[1,512,2048]{2,1,0:T(8,128)(2,1)} %param.30) | copy-start | bytes 6291460
  6.5 78.2 %all-gather.5.cloned.1.call-start = ((), (), s32[]{:S(2)}) async-start(), calls=%async_computation.8 | async-start | bytes 3932160 | tf_op jit(solution)/shard_map/all_gather | solution.py:97
  7.4 7.7 %collective-permute-start.1 = (bf16[8,128]{1,0:T(8,128)(2,1)S(1)}, bf16[8,128]{1,0:T(8,128)(2,1)S(1)}, u32[]{:S(2)}, u32[]{:S(2)}) collective-permute-start(bf16[8,128]{1,0:T(8,128)(2,1)S(1)} %get-tuple-element.26), channel_id=1, source_target_pairs={{4,0},{8,4},{12,8},{16,12},{20,16},{24,20},{28,24},{5,1},{9,5},{13... | collective-permute-start | bytes 6152 | tf_op jit(solution)/shard_map/ppermute | solution.py:21
  8.7 6.8 %collective-permute-start = (bf16[8,128]{1,0:T(8,128)(2,1)S(1)}, bf16[8,128]{1,0:T(8,128)(2,1)S(1)}, u32[]{:S(2)}, u32[]{:S(2)}) collective-permute-start(bf16[8,128]{1,0:T(8,128)(2,1)S(1)} %get-tuple-element.25), channel_id=1, source_target_pairs={{0,4},{4,8},{8,12},{12,16},{16,20},{20,24},{24,28},{1,5},{5,9},{9,... | collective-permute-start | bytes 6152 | tf_op jit(solution)/shard_map/ppermute | solution.py:20
  16.3 9.1 %copy-start.2 = (bf16[512,2048]{1,0:T(8,128)(2,1)S(1)}, bf16[512,2048]{1,0:T(8,128)(2,1)}, u32[]{:S(2)}) copy-start(bf16[512,2048]{1,0:T(8,128)(2,1)} %param.20) | copy-start | bytes 6291460
  16.3 9.1 %copy-start.7 = (f32[512]{0:T(512)S(1)}, f32[512]{0:T(512)}, u32[]{:S(2)}) copy-start(f32[512]{0:T(512)} %param.19) | copy-start | bytes 6148
  25.4 1.2 copy-start.3
  25.4 1.2 copy-start.6
  26.7 1.9 copy-start.4
  27.2 1.3 copy-start.1
  57.0 57.8 %all-gather.3.cloned.1.call-start = ((), (), s32[]{:S(2)}) async-start(), calls=%async_computation.6 | async-start | bytes 3932160 | tf_op jit(solution)/shard_map/all_gather | solution.py:97
  83.0 72.2 %reduce-scatter.5.cloned.1.call-start = ((), (), s32[]{:S(2)}) async-start(), calls=%async_computation.9 | async-start | bytes 3932160 | tf_op jit(solution)/shard_map/reduce_scatter | solution.py:112
  84.8 5.6 %copy-start.10 = (f32[1,512]{1,0:T(1,128)S(1)}, f32[1,512]{1,0:T(1,128)}, u32[]{:S(2)}) copy-start(f32[1,512]{1,0:T(1,128)} %param.28) | copy-start | bytes 6148
  84.8 5.6 %copy-start.11 = (f32[1,512]{1,0:T(1,128)S(1)}, f32[1,512]{1,0:T(1,128)}, u32[]{:S(2)}) copy-start(f32[1,512]{1,0:T(1,128)} %param.29) | copy-start | bytes 6148
  99.1 96.1 %reduce-scatter.3.cloned.1.call-start = ((), (), s32[]{:S(2)}) async-start(), calls=%async_computation.7 | async-start | bytes 3932160 | tf_op jit(solution)/shard_map/reduce_scatter | solution.py:112
  129.4 71.4 %copy-start.5 = (s32[256,4]{0,1:T(4,128)S(1)}, s32[256,4]{0,1:T(4,128)}, u32[]{:S(2)}) copy-start(s32[256,4]{0,1:T(4,128)} %param.24) | copy-start | bytes 12292
  129.4 71.4 %copy-start.8 = (f32[256,4]{0,1:T(4,128)S(1)}, f32[256,4]{0,1:T(4,128)}, u32[]{:S(2)}) copy-start(f32[256,4]{0,1:T(4,128)} %param.25) | copy-start | bytes 12292
  155.1 40.1 %all-to-all-start.3 = ((bf16[8,96,512]{2,1,0:T(8,128)(2,1)}), bf16[8,96,512]{2,1,0:T(8,128)(2,1)S(1)}, u32[]{:S(2)}, u32[]{:S(2)}) async-start(bf16[8,96,512]{2,1,0:T(8,128)(2,1)} %reduce-scatter.5.cloned.1.call-done), calls=%async_computation.5 | async-start | bytes 1572864 | tf_op jit(solution)/shard_map/all_to_all | solution.py:113
  195.3 25.7 %all-to-all-start.1 = ((bf16[8,96,512]{2,1,0:T(8,128)(2,1)}), bf16[8,96,512]{2,1,0:T(8,128)(2,1)}, u32[]{:S(2)}, u32[]{:S(2)}) async-start(bf16[8,96,512]{2,1,0:T(8,128)(2,1)} %reduce-scatter.3.cloned.1.call-done), calls=%async_computation.2 | async-start | bytes 1572864 | tf_op jit(solution)/shard_map/all_to_all | solution.py:113
  201.8 28.4 %copy-start.9 = (f32[512]{0:T(512)S(1)}, f32[512]{0:T(512)}, u32[]{:S(2)}) copy-start(f32[512]{0:T(512)} %param.31) | copy-start | bytes 6148
Sparse Core Ops, SparseCore 0:
  57.2 27.5 all-gather.4
  86.3 28.4 all-gather.2
  117.4 37.7 reduce-scatter.4
  157.5 37.7 reduce-scatter.2
where the time goes:
time: 239 us
  waiting for transfers between devices  97.4 us (41%)
  blocking collectives  64 us (27%)
  matrix products  39.2 us (16%)
  starting transfers between devices  17.9 us (7%)
  between operations  13.3 us (6%)
  other arithmetic  4.21 us (2%)
  local copies, waits for them, and re-layouts  2.53 us (1%)
    reduce_scatter x2, waiting for transfers between devices, expert(): lax.psum_scatter(partial_value, 'tp', scatter_dimension=2, tiled=True)  60.3 us
    all_to_all x2, blocking collectives, dispatched(): lax.all_to_all(own_slots, 'sp', split_axis=0, concat_axis=0, tiled=True)  51.7 us
    all_to_all x2, waiting for transfers between devices, expert(): return lax.all_to_all(summed, 'sp', split_axis=0, concat_axis=0, tiled=True)  19.2 us
    dot_general x2, matrix products, expert(): jnp.dot(activation, w_down[0], preferred_element_type=jnp.float32)  17.8 us
    all_gather x2, waiting for transfers between devices, dispatched(): return lax.all_gather(arrived, 'tp', axis=1, tiled=True)  17.4 us
    dot_general x2, matrix products, expert(): jnp.dot(row_block, w_gate[0], preferred_element_type=jnp.float32)  11.1 us
    all_to_all x2, starting transfers between devices, expert(): return lax.all_to_all(summed, 'sp', split_axis=0, concat_axis=0, tiled=True)  11 us
    all_gather x1, blocking collectives, shards(): all_groups = lax.all_gather(pool_out, 'tp', axis=1, tiled=True)  6.3 us
  transfers between devices with their start and end apart: 8, of which 6 were waited for; matrix products, arithmetic and copies ran while one was open for 14% of the time, Pallas kernels for 0%

commit v1 on v0

--- a/solution.py
+++ b/solution.py
@@ -1,7 +1,13 @@
+import functools
+
 import jax
 import jax.numpy as jnp
 from jax import lax
+from jax.experimental import pallas as pl
+from jax.experimental.pallas import tpu as pltpu
 from jax.sharding import PartitionSpec as P
+
+MESH = pl.DeviceIdType.MESH
 
 epsilon = 1e-06
 reach_rows = 8
@@ -27,7 +33,7 @@
     return values * lax.rsqrt(jnp.mean(values * values, axis=-1, keepdims=True) + epsilon)
 
 
-def shards(
+def routed_shards(
     pool_in,
     pool_weight,
     pool_scale,
@@ -136,6 +142,697 @@
     return (own_cols + combined * row_scale[:, None] * expert_norm).astype(jnp.bfloat16)
 
 
+x_size = 2
+core_count = 2
+first_rows = 48
+vmem_limit = 60 * 1024 * 1024
+UP, DOWN, ACROSS, SIBLING = range(4)
+XF, ZF = range(2)
+
+
+def layer_kernel(
+    nz,
+    pool_in,
+    pool_weight,
+    pool_scale,
+    pool_norm,
+    out_weight_hbm,
+    stream_hbm,
+    mix_norm,
+    ffn_norm,
+    routes,
+    route_weights,
+    w_gate_hbm,
+    w_up_hbm,
+    gate_bias,
+    up_bias,
+    w_down_hbm,
+    expert_norm,
+    out_ref,
+    tokens,
+    w_gate,
+    w_up,
+    w_down,
+    out_weight,
+    stream,
+    pool_all,
+    pool_edges,
+    weight_all,
+    scale_all,
+    padded,
+    normed,
+    mix_out,
+    mixed,
+    route_all,
+    hidden,
+    parts,
+    parts_in,
+    pair_out,
+    pair_keep,
+    pair_in,
+    side_out,
+    side_in,
+    total,
+    far_out,
+    far_in,
+    squares,
+    load_sem,
+    ag_send,
+    ag_recv,
+    front_send,
+    front_recv,
+    edge_send,
+    edge_recv,
+    route_send,
+    route_recv,
+    part_send,
+    part_recv,
+    pair_send,
+    pair_recv,
+    side_send,
+    side_recv,
+    far_send,
+    far_recv,
+    sq_send,
+    sq_recv,
+):
+    sp, tp = lax.axis_index("sp"), lax.axis_index("tp")
+    n_sp = nz * x_size
+    n_tp = pool_all.shape[0]
+    z, x = sp // x_size, sp % x_size
+    y, core = tp // core_count, tp % core_count
+    rows, width = stream.shape
+    cols = out_ref.shape[1]
+    group_width = pool_in.shape[1]
+    half_rows = rows // core_count
+    sibling = y * core_count + (1 - core)
+    opposite = (1 - y) * core_count + core
+    far_z = nz - 1
+
+    def remote(src, dst, send, recv, to_sp, to_tp):
+        return pltpu.make_async_remote_copy(
+            src_ref=src,
+            dst_ref=dst,
+            send_sem=send,
+            recv_sem=recv,
+            device_id=(to_sp, to_tp),
+            device_id_type=MESH,
+        )
+
+    loads = [
+        pltpu.make_async_copy(src, dst, load_sem.at[i])
+        for i, (src, dst) in enumerate(
+            (
+                (out_weight_hbm, out_weight),
+                (stream_hbm, stream),
+                (w_gate_hbm.at[0], w_gate),
+                (w_up_hbm.at[0], w_up),
+                (w_down_hbm.at[0], w_down),
+            )
+        )
+    ]
+    for load in loads:
+        load.start()
+
+    barrier = pltpu.get_barrier_semaphore()
+
+    def greet(to_sp, to_tp):
+        pl.semaphore_signal(barrier, inc=1, device_id=(to_sp, to_tp), device_id_type=MESH)
+
+    for d in range(1, n_sp):
+        greet((sp + d) % n_sp, tp)
+    for d in range(1, n_tp):
+        greet(sp, (tp + d) % n_tp)
+
+    @pl.when(sp > 0)
+    def _():
+        for d in range(1, n_tp):
+            greet(sp - 1, (tp + d) % n_tp)
+
+    @pl.when(sp < n_sp - 1)
+    def _():
+        for d in range(1, n_tp):
+            greet(sp + 1, (tp + d) % n_tp)
+
+    near = (sp > 0).astype(jnp.int32) + (sp < n_sp - 1).astype(jnp.int32)
+    pl.semaphore_wait(barrier, (n_sp - 1) + (n_tp - 1) * (1 + near))
+
+    edge = pool_edges.shape[2]
+
+    def edge_copy(side, to_tp, d):
+        src = pool_in.at[pl.ds(rows - edge, edge)] if side == 0 else pool_in.at[pl.ds(0, edge)]
+        return remote(
+            src,
+            pool_edges.at[tp, side],
+            edge_send.at[side, d],
+            edge_recv.at[tp, side],
+            sp + 1 if side == 0 else sp - 1,
+            to_tp,
+        )
+
+    def edge_loop(side, act):
+        @pl.when(sp < n_sp - 1 if side == 0 else sp > 0)
+        def _():
+            for d in range(n_tp):
+                act(edge_copy(side, (tp + d) % n_tp, d))
+
+    for side in range(2):
+        edge_loop(side, lambda copy: copy.start())
+
+    def front_copies(d):
+        to = (tp + d) % n_tp
+        return [
+            remote(pool_in, pool_all.at[tp], front_send.at[d, 0], front_recv.at[tp, 0], sp, to),
+            remote(
+                pool_weight.at[0], weight_all.at[tp], front_send.at[d, 1], front_recv.at[tp, 1], sp, to
+            ),
+            remote(pool_scale, scale_all.at[tp], front_send.at[d, 2], front_recv.at[tp, 2], sp, to),
+        ]
+
+    for d in range(1, n_tp):
+        for copy in front_copies(d):
+            copy.start()
+    pool_all[tp] = pool_in[...]
+    weight_all[tp] = pool_weight[0]
+    scale_all[tp] = pool_scale[...]
+
+    lanes = lax.broadcasted_iota(jnp.int32, (rows, 128), 1)
+    by_expert = jnp.zeros((rows, 128), jnp.float32)
+    for k in range(routes.shape[1]):
+        by_expert += jnp.where(routes[:, k : k + 1] == lanes, route_weights[:, k : k + 1], 0.0)
+    route_rows = route_all.shape[1]
+    route_all[sp] = by_expert.T[:route_rows]
+
+    def route_copy(d):
+        to = (sp + d) % n_sp
+        return remote(
+            route_all.at[sp], route_all.at[sp], route_send.at[d], route_recv.at[sp], to, tp
+        )
+
+    for d in range(1, n_sp):
+        route_copy(d).start()
+
+    for d in range(1, n_tp):
+        src_tp = (tp + d) % n_tp
+        for i, (src, dst) in enumerate(
+            (
+                (pool_in, pool_all),
+                (pool_weight.at[0], weight_all),
+                (pool_scale, scale_all),
+            )
+        ):
+            remote(
+                src, dst.at[src_tp], front_send.at[d, i], front_recv.at[src_tp, i], sp, src_tp
+            ).wait_recv()
+
+    @pl.when(sp > 0)
+    def _():
+        for g in range(n_tp):
+            remote(
+                pool_in.at[pl.ds(0, edge)],
+                pool_edges.at[g, 0],
+                edge_send.at[0, 0],
+                edge_recv.at[g, 0],
+                sp - 1,
+                tp,
+            ).wait_recv()
+            padded[g, 0:reach_rows, :] = pool_edges[g, 0].astype(jnp.float32)[edge - reach_rows :]
+
+    @pl.when(sp == 0)
+    def _():
+        padded[:, 0:reach_rows, :] = jnp.zeros((n_tp, reach_rows, group_width), jnp.float32)
+
+    @pl.when(sp < n_sp - 1)
+    def _():
+        for g in range(n_tp):
+            remote(
+                pool_in.at[pl.ds(0, edge)],
+                pool_edges.at[g, 1],
+                edge_send.at[0, 0],
+                edge_recv.at[g, 1],
+                sp + 1,
+                tp,
+            ).wait_recv()
+            padded[g, reach_rows + rows :, :] = pool_edges[g, 1].astype(jnp.float32)[:reach_rows]
+
+    @pl.when(sp == n_sp - 1)
+    def _():
+        padded[:, reach_rows + rows :, :] = jnp.zeros((n_tp, reach_rows, group_width), jnp.float32)
+
+    positions = sp * rows + lax.broadcasted_iota(jnp.int32, (rows, group_width), 0)
+    mean_square = jnp.zeros((rows, 1), jnp.float32)
+    for g in range(n_tp):
+        radius = 1 << g
+        values = pool_all[g].astype(jnp.float32)
+        padded[g, reach_rows : reach_rows + rows, :] = values
+        window_sum = values
+        for offset in range(1, radius + 1):
+            window_sum += padded[g, reach_rows + offset : reach_rows + offset + rows, :]
+            window_sum += padded[g, reach_rows - offset : reach_rows - offset + rows, :]
+        last = jnp.minimum(positions + radius, n_sp * rows - 1)
+        counts = last - jnp.maximum(positions - radius, 0) + 1
+        deviation = (window_sum / counts.astype(jnp.float32) - values).astype(jnp.bfloat16)
+        pool_out = (
+            jnp.dot(deviation, weight_all[g], preferred_element_type=jnp.float32) * scale_all[g]
+        ).astype(jnp.bfloat16)
+        normed[:, g * group_width : (g + 1) * group_width] = pool_out
+        wide = pool_out.astype(jnp.float32)
+        mean_square += jnp.sum(wide * wide, axis=1, keepdims=True)
+    pool_width = n_tp * group_width
+    row_scale = lax.rsqrt(mean_square / pool_width + epsilon)
+    normed[...] = (normed[...].astype(jnp.float32) * row_scale * pool_norm[...]).astype(jnp.bfloat16)
+
+    for load in loads[:2]:
+        load.wait()
+    for t in range(width // cols):
+        mix_out[:, t * cols : (t + 1) * cols] = jnp.dot(
+            normed[...], out_weight[:, t * cols : (t + 1) * cols], preferred_element_type=jnp.float32
+        )
+
+    tile = 32
+
+    def mix_rows(i, carry):
+        part = pl.ds(pl.multiple_of(i * tile, tile), tile)
+        value = mix_out[part, :]
+        scaled = value * lax.rsqrt(jnp.mean(value * value, axis=1, keepdims=True) + epsilon)
+        summed = (stream[part, :].astype(jnp.float32) + scaled * mix_norm[...]).astype(jnp.bfloat16)
+        mixed[part, :] = summed
+        wide = summed.astype(jnp.float32)
+        wide = wide * lax.rsqrt(jnp.mean(wide * wide, axis=1, keepdims=True) + epsilon)
+        tokens[sp, part, :] = (wide * ffn_norm[...]).astype(jnp.bfloat16)
+        return carry
+
+    lax.fori_loop(0, rows // tile, mix_rows, 0)
+
+    def piece(block, kind, whose):
+        start = whose * half_rows + (0 if kind == XF else first_rows)
+        count = first_rows if kind == XF else half_rows - first_rows
+        return tokens.at[block, pl.ds(pl.multiple_of(start, 16), count), :]
+
+    def ag_copy(block, kind, way):
+        to_sp = {UP: sp + x_size, DOWN: sp - x_size, ACROSS: z * x_size + (1 - x), SIBLING: sp}[way]
+        recv = ag_recv.at[block, kind + (2 if way == SIBLING else 0)]
+        ref = piece(block, kind, core)
+        return remote(
+            ref, ref, ag_send.at[block, kind, way], recv, to_sp, sibling if way == SIBLING else tp
+        )
+
+    def ag_arrived(block, kind, from_sibling):
+        whose = 1 - core if from_sibling else core
+        ref = piece(block, kind, whose)
+        recv = ag_recv.at[block, kind + (2 if from_sibling else 0)]
+        remote(ref, ref, ag_send.at[block, kind, SIBLING], recv, sp, sibling).wait_recv()
+
+    def ag_ways(zc, col_is_own, kind, act):
+        block = zc * x_size + (x if col_is_own else 1 - x)
+        along = col_is_own or kind == XF
+
+        if along:
+
+            @pl.when((zc <= z) & (z < far_z))
+            def _():
+                act(ag_copy(block, kind, UP))
+
+            @pl.when((zc >= z) & (z > 0))
+            def _():
+                act(ag_copy(block, kind, DOWN))
+
+        if col_is_own and kind == ZF:
+            act(ag_copy(block, kind, ACROSS))
+        if col_is_own and kind == XF:
+
+            @pl.when(zc == z)
+            def _():
+                act(ag_copy(block, kind, ACROSS))
+
+        if col_is_own:
+
+            @pl.when(zc != z)
+            def _():
+                act(ag_copy(block, kind, SIBLING))
+
+        else:
+            act(ag_copy(block, kind, SIBLING))
+
+    def start(copy):
+        copy.start()
+
+    def take(zc, col_is_own, kind):
+        block = zc * x_size + (x if col_is_own else 1 - x)
+        ag_arrived(block, kind, False)
+        ag_ways(zc, col_is_own, kind, start)
+
+    def take_set(zc):
+        take(zc, True, ZF)
+        take(zc, True, XF)
+        take(zc, False, XF)
+        take(zc, False, ZF)
+
+    ag_ways(z, True, XF, start)
+    ag_ways(z, True, ZF, start)
+
+    for d in range(1, n_sp):
+        src_sp = (sp + d) % n_sp
+        remote(
+            route_all.at[sp], route_all.at[src_sp], route_send.at[d], route_recv.at[src_sp], src_sp, tp
+        ).wait_recv()
+    for load in loads[2:]:
+        load.wait()
+
+    upper = z >= (nz + 1) // 2
+    low_z = jnp.where(upper, far_z - z, z)
+
+    def plane_at(step):
+        plane = jnp.where(step <= low_z, low_z - step, step)
+        return jnp.where(upper, far_z - plane, plane)
+
+    n_hidden = hidden.shape[1]
+    hidden_tile = min(256, n_hidden)
+
+    def part_copy(block, q_y):
+        q = q_y * core_count + (1 - core)
+        return remote(
+            parts.at[block, q],
+            parts_in.at[block, q_y],
+            part_send.at[block, q_y],
+            part_recv.at[block, q_y],
+            sp,
+            sibling,
+        )
+
+    def pair_copy(block):
+        return remote(
+            pair_out.at[block], pair_in.at[block], pair_send.at[block], pair_recv.at[block], sp, opposite
+        )
+
+    def side_copy(zc):
+        return remote(
+            side_out.at[zc],
+            side_in.at[zc],
+            side_send.at[zc],
+            side_recv.at[zc],
+            z * x_size + (1 - x),
+            tp,
+        )
+
+    def far_copy(zc):
+        return remote(
+            far_out.at[zc], far_in.at[z], far_send.at[zc], far_recv.at[z], zc * x_size + x, tp
+        )
+
+    def compute(block):
+        own_row = lax.broadcasted_iota(jnp.int32, (route_rows, rows), 0) == sp
+        weight = jnp.sum(jnp.where(own_row, route_all[block], 0.0), axis=0, keepdims=True)
+        weight = jnp.broadcast_to(weight, (128, rows)).T
+        for j in range(n_hidden // hidden_tile):
+            span = slice(j * hidden_tile, (j + 1) * hidden_tile)
+            data = tokens[block]
+            gate = jnp.dot(data, w_gate[:, span], preferred_element_type=jnp.float32)
+            up = jnp.dot(data, w_up[:, span], preferred_element_type=jnp.float32)
+            gate_cut = jnp.minimum(gate + gate_bias[:, span], clamp_limit)
+            up_cut = jnp.clip(up + up_bias[:, span], -clamp_limit, clamp_limit)
+            active = (up_cut + 1.0) * (gate_cut * jax.nn.sigmoid(sigmoid_alpha * gate_cut))
+            for i in range(hidden_tile // 128):
+                lane = slice(i * 128, (i + 1) * 128)
+                at = j * hidden_tile + i * 128
+                hidden[:, at : at + 128] = (active[:, lane] * weight).astype(jnp.bfloat16)
+
+        def down(i, carry):
+            whose = jnp.where(i < 2, 1 - core, core)
+            q = (i % 2) * core_count + whose
+            at = pl.ds(pl.multiple_of(q * cols, cols), cols)
+            parts[block, q] = jnp.dot(
+                hidden[...], w_down[:, at], preferred_element_type=jnp.float32
+            ).astype(jnp.bfloat16)
+
+            @pl.when(i < 2)
+            def _():
+                part_copy(block, i % 2).start()
+
+            return carry
+
+        lax.fori_loop(0, n_tp, down, 0)
+
+    def join_cores(block):
+        for q_y in range(n_tp // core_count):
+            part_copy(block, q_y).wait_recv()
+        away = parts[block, opposite].astype(jnp.float32) + parts_in[block, 1 - y].astype(jnp.float32)
+        pair_out[block] = away.astype(jnp.bfloat16)
+        pair_copy(block).start()
+        pair_keep[block] = parts[block, tp].astype(jnp.float32) + parts_in[block, y].astype(
+            jnp.float32
+        )
+
+    def join_pair_other(step):
+        zc = plane_at(step)
+        block = zc * x_size + (1 - x)
+        pair_copy(block).wait_recv()
+        side_out[zc] = (pair_keep[block] + pair_in[block].astype(jnp.float32)).astype(jnp.bfloat16)
+        side_copy(zc).start()
+
+    def join_pair_own(step):
+        zc = plane_at(step)
+        block = zc * x_size + x
+        pair_copy(block).wait_recv()
+        total[zc] = pair_keep[block] + pair_in[block].astype(jnp.float32)
+
+    def join_sides(step):
+        zc = plane_at(step)
+        side_copy(zc).wait_recv()
+        value = total[zc] + side_in[zc].astype(jnp.float32)
+        total[zc] = value
+
+        @pl.when(zc != z)
+        def _():
+            far_out[zc] = value.astype(jnp.bfloat16)
+            far_copy(zc).start()
+
+    def step_body(step, carry):
+        zc = plane_at(step)
+        inner = low_z > 0
+
+        @pl.when((step >= 1) & ((step != 2) | (low_z == 0)))
+        def _():
+            take_set(zc)
+
+        if nz > 2:
+
+            @pl.when((step == 1) & inner)
+            def _():
+                take_set(plane_at(2))
+
+        col = jnp.where(step == 0, x, 1 - x)
+        first, second = zc * x_size + col, zc * x_size + (1 - col)
+
+        @pl.when(step >= 1)
+        def _():
+            ag_arrived(first, XF, True)
+            ag_arrived(first, ZF, True)
+
+        compute(first)
+        join_cores(first)
+
+        @pl.when(step == 0)
+        def _():
+            take(z, False, XF)
+            take(z, False, ZF)
+
+        @pl.when(step >= 1)
+        def _():
+            join_pair_other(step - 1)
+            join_pair_own(step - 1)
+
+        @pl.when(step >= 2)
+        def _():
+            join_sides(step - 2)
+
+        ag_arrived(second, XF, True)
+        ag_arrived(second, ZF, True)
+        compute(second)
+        join_cores(second)
+        return carry
+
+    lax.fori_loop(0, nz, step_body, 0)
+    join_pair_other(nz - 1)
+    if nz > 1:
+        join_sides(nz - 2)
+    join_pair_own(nz - 1)
+    join_sides(nz - 1)
+
+    combined = total[z]
+    for d in range(1, nz):
+        src_z = (z + d) % nz
+        remote(
+            far_out.at[src_z],
+            far_in.at[src_z],
+            far_send.at[src_z],
+            far_recv.at[src_z],
+            src_z * x_size + x,
+            tp,
+        ).wait_recv()
+        combined += far_in[src_z].astype(jnp.float32)
+    total[z] = combined
+
+    own_squares = jnp.sum(combined * combined, axis=1, keepdims=True)
+    squares[tp] = jnp.broadcast_to(own_squares, (rows, 128)).T[:8]
+
+    def squares_copy(d):
+        return remote(
+            squares.at[tp], squares.at[tp], sq_send.at[d], sq_recv.at[tp], sp, (tp + d) % n_tp
+        )
+
+    for d in range(1, n_tp):
+        squares_copy(d).start()
+    summed = squares[tp]
+    for d in range(1, n_tp):
+        src_tp = (tp + d) % n_tp
+        remote(
+            squares.at[tp], squares.at[src_tp], sq_send.at[d], sq_recv.at[src_tp], sp, src_tp
+        ).wait_recv()
+        summed += squares[src_tp]
+    row_scale = lax.rsqrt(summed[:1] / width + epsilon)
+    row_scale = jnp.broadcast_to(row_scale, (128, rows)).T
+    for i in range(cols // 128):
+        lane = slice(i * 128, (i + 1) * 128)
+        own = mixed[:, pl.ds(pl.multiple_of(tp * cols + i * 128, 128), 128)].astype(jnp.float32)
+        out_ref[:, lane] = (own + total[z, :, lane] * row_scale * expert_norm[:, lane]).astype(
+            jnp.bfloat16
+        )
+
+    def sent(copy):
+        copy.wait_send()
+
+    for side in range(2):
+        edge_loop(side, sent)
+    for d in range(1, n_tp):
+        for copy in front_copies(d):
+            sent(copy)
+        sent(squares_copy(d))
+    for d in range(1, n_sp):
+        sent(route_copy(d))
+
+    def all_sent(zc, carry):
+        for col_is_own in (True, False):
+            for kind in (XF, ZF):
+                ag_ways(zc, col_is_own, kind, sent)
+        for i in range(x_size):
+            block = zc * x_size + i
+            for q_y in range(n_tp // core_count):
+                sent(part_copy(block, q_y))
+            sent(pair_copy(block))
+        sent(side_copy(zc))
+
+        @pl.when(zc != z)
+        def _():
+            sent(far_copy(zc))
+
+        return carry
+
+    lax.fori_loop(0, nz, all_sent, 0)
+
+
+def gathered_shards(*args):
+    pool_in, pool_norm, out_weight, stream = args[0], args[3], args[4], args[5]
+    w_gate, w_down = args[10], args[14]
+    n_sp, n_tp = lax.axis_size("sp"), lax.axis_size("tp")
+    nz = n_sp // x_size
+    rows, width = stream.shape
+    n_hidden = w_gate.shape[2]
+    cols = width // n_tp
+    group_width = pool_in.shape[1]
+    bf16, f32 = jnp.bfloat16, jnp.float32
+    row_args = (2, 3, 6, 7, 15)
+    args = [a.reshape(1, -1) if i in row_args else a for i, a in enumerate(args)]
+    in_hbm = (4, 5, 10, 11, 14)
+    in_specs = [
+        pl.BlockSpec(memory_space=pl.ANY if i in in_hbm else pltpu.VMEM) for i in range(len(args))
+    ]
+    edge = 2 * reach_rows
+    route_rows = -(-n_sp // 8) * 8
+    dma = pltpu.SemaphoreType.DMA
+    scratch = [
+        pltpu.VMEM((n_sp, rows, width), bf16),
+        pltpu.VMEM((width, n_hidden), bf16),
+        pltpu.VMEM((width, n_hidden), bf16),
+        pltpu.VMEM((n_hidden, width), bf16),
+        pltpu.VMEM(out_weight.shape, bf16),
+        pltpu.VMEM((rows, width), bf16),
+        pltpu.VMEM((n_tp, rows, group_width), bf16),
+        pltpu.VMEM((n_tp, 2, edge, group_width), bf16),
+        pltpu.VMEM((n_tp, group_width, group_width), bf16),
+        pltpu.VMEM((n_tp, 1, group_width), f32),
+        pltpu.VMEM((n_tp, rows + 2 * reach_rows, group_width), f32),
+        pltpu.VMEM((rows, n_tp * group_width), bf16),
+        pltpu.VMEM((rows, width), f32),
+        pltpu.VMEM((rows, width), bf16),
+        pltpu.VMEM((n_sp, route_rows, rows), f32),
+        pltpu.VMEM((rows, n_hidden), bf16),
+        pltpu.VMEM((n_sp, n_tp, rows, cols), bf16),
+        pltpu.VMEM((n_sp, n_tp // core_count, rows, cols), bf16),
+        pltpu.VMEM((n_sp, rows, cols), bf16),
+        pltpu.VMEM((n_sp, rows, cols), f32),
+        pltpu.VMEM((n_sp, rows, cols), bf16),
+        pltpu.VMEM((nz, rows, cols), bf16),
+        pltpu.VMEM((nz, rows, cols), bf16),
+        pltpu.VMEM((nz, rows, cols), f32),
+        pltpu.VMEM((nz, rows, cols), bf16),
+        pltpu.VMEM((nz, rows, cols), bf16),
+        pltpu.VMEM((n_tp, 8, rows), f32),
+        dma((5,)),
+        dma((n_sp, 2, 4)),
+        dma((n_sp, 4)),
+        dma((n_tp, 3)),
+        dma((n_tp, 3)),
+        dma((2, n_tp)),
+        dma((n_tp, 2)),
+        dma((n_sp,)),
+        dma((n_sp,)),
+        dma((n_sp, n_tp // core_count)),
+        dma((n_sp, n_tp // core_count)),
+        dma((n_sp,)),
+        dma((n_sp,)),
+        dma((nz,)),
+        dma((nz,)),
+        dma((nz,)),
+        dma((nz,)),
+        dma((n_tp,)),
+        dma((n_tp,)),
+    ]
+    return pl.pallas_call(
+        functools.partial(layer_kernel, nz),
+        out_shape=jax.ShapeDtypeStruct((rows, cols), bf16),
+        in_specs=in_specs,
+        out_specs=pl.BlockSpec(memory_space=pltpu.VMEM),
+        scratch_shapes=scratch,
+        compiler_params=pltpu.CompilerParams(
+            collective_id=0, has_side_effects=True, vmem_limit_bytes=vmem_limit
+        ),
+        name="layer",
+    )(*args)
+
+
+def shards(*args):
+    pool_in, out_weight, stream, w_gate = args[0], args[4], args[5], args[10]
+    n_sp, n_tp = lax.axis_size("sp"), lax.axis_size("tp")
+    rows, width = stream.shape
+    cols, n_hidden = width // n_tp, w_gate.shape[2]
+    slots = n_sp * rows * (2 * width + (2 + 1 + 1 + 2 + 1) * 2 * cols + 2 * width + 2 * width)
+    fixed = 2 * (3 * width * n_hidden + out_weight.size) + 10 * rows * width
+    fits = slots + fixed < vmem_limit * 9 // 10
+    shaped = (
+        n_tp == 2 * core_count
+        and n_sp % x_size == 0
+        and w_gate.shape[0] == 1
+        and rows % 128 == 0
+        and rows // core_count > first_rows
+        and cols % 128 == 0
+        and n_hidden % 256 == 0
+        and pool_in.shape[1] == 128
+        and n_sp <= 128
+    )
+    return (gathered_shards if fits and shaped else routed_shards)(*args)
+
+
 def solution(mesh):
     in_specs = (
         P("sp", "tp"),

time: 239 us -> 127 us (0.53)
  Pallas kernels: 0 us -> 122 us
  waiting for transfers between devices: 97.4 us -> 0 us
  blocking collectives: 64 us -> 0 us
  matrix products: 39.2 us -> 0 us
  starting transfers between devices: 17.9 us -> 0 us
  between operations: 13.3 us -> 0.01 us
  other arithmetic: 4.21 us -> 0 us
    pallas_call x0 -> x1, Pallas kernels: none -> 122 us  [gathered_shards(): pl.pallas_call(functools.partial(layer_kernel, nz), out_shape=jax.ShapeDt...]
    reduce_scatter x2 -> x0, waiting for transfers between devices: 60.3 us -> none  [expert(): lax.psum_scatter(partial_value, 'tp', scatter_dimension=2, tiled=True)]
    all_to_all x2 -> x0, blocking collectives: 51.7 us -> none  [dispatched(): lax.all_to_all(own_slots, 'sp', split_axis=0, concat_axis=0, tiled=True)]
    dot_general x13 -> x0, matrix products: 39.2 us -> none  [the longest x2 17.8 us: expert(): jnp.dot(activation, w_down[0], preferred_element_type=jnp.float32)]
    all_to_all x2 -> x0, waiting for transfers between devices: 19.2 us -> none  [expert(): return lax.all_to_all(summed, 'sp', split_axis=0, concat_axis=0, tiled=True)]
    all_gather x2 -> x0, waiting for transfers between devices: 17.4 us -> none  [dispatched(): return lax.all_gather(arrived, 'tp', axis=1, tiled=True)]
    all_to_all x2 -> x0, starting transfers between devices: 11 us -> none  [expert(): return lax.all_to_all(summed, 'sp', split_axis=0, concat_axis=0, tiled=True)]
    ppermute x2 -> x0, starting transfers between devices: 6.78 us -> none  [the longest x1 5.5 us: extended_2(): before = lax.ppermute(last, axis, up)]
  transfers between devices with their start and end apart: 8 -> 0, of which waited for: 6 -> 0; matrix products, arithmetic and copies ran while one was open for 14% -> 0% of each run, Pallas kernels for 0% -> 0%
where the time goes in v1:
time: 127 us
  Pallas kernels  122 us (96%)
  local copies, waits for them, and re-layouts  4.63 us (4%)
    pallas_call x1, Pallas kernels, gathered_shards(): pl.pallas_call(functools.partial(layer_kernel, nz), out_shape=jax.ShapeDt...  122 us
    unnamed x3, local copies, waits for them, and re-layouts  4.63 us

profile of v1, /device:TPU:0, one launch (start us, length us, event | category | flops | bytes accessed | tf_op | source)
XLA Modules:
  0.0 127.1 jit_solution(9522447260144475931)
XLA Ops:
  0.0 1.5 %copy.17.routes = s32[256,4]{1,0:T(8,128)} copy(s32[256,4]{0,1:T(4,128)} %param.24) | data formatting | bytes 8192 | tf_op args[8]
  1.5 1.5 %copy.18.route_weights = f32[256,4]{1,0:T(8,128)} copy(f32[256,4]{0,1:T(4,128)} %param.25) | data formatting | bytes 8192 | tf_op args[9]
  3.0 122.4 %layer.1 = bf16[256,512]{1,0:T(8,128)(2,1)} custom-call(bf16[256,128]{1,0:T(8,128)(2,1)} %pool_in.1, bf16[1,128,128]{2,1,0:T(8,128)(2,1)} %pool_weight.1, f32[1,128]{1,0:T(1,128)} %bitcast.9, f32[1,512]{1,0:T(1,128)} %bitcast.7, bf16[512,2048]{1,0:T(8,128)(2,1)} %out_weight_hbm.1, bf16[256,2048]{1,0:T(8,128)(2,1)} %stream_hbm.1, f32[1,2048]{1,0:T(1,128)} %bitcast.5, ...), custom_call_target="tpu_custom_call" | custom-call | tf_op jit(solution)/shard_map/layer/pallas_call | solution.py:801
  125.4 1.7 %copy.20 = bf16[256,512]{1,0:T(8,128)(2,1)} copy(bf16[256,512]{1,0:T(8,128)(2,1)} %layer.1) | data formatting | bytes 524288

commit v2 on v1

--- a/solution.py
+++ b/solution.py
@@ -144,7 +144,8 @@
 
 x_size = 2
 core_count = 2
-first_rows = 48
+halves = 2
+first_share = 8, 3
 vmem_limit = 60 * 1024 * 1024
 UP, DOWN, ACROSS, SIBLING = range(4)
 XF, ZF = range(2)
@@ -224,7 +225,9 @@
     rows, width = stream.shape
     cols = out_ref.shape[1]
     group_width = pool_in.shape[1]
-    half_rows = rows // core_count
+    half_rows = rows // halves
+    core_rows = half_rows // core_count
+    first_cols = width * first_share[1] // first_share[0]
     sibling = y * core_count + (1 - core)
     opposite = (1 - y) * core_count + core
     far_z = nz - 1
@@ -316,12 +319,12 @@
     weight_all[tp] = pool_weight[0]
     scale_all[tp] = pool_scale[...]
 
-    lanes = lax.broadcasted_iota(jnp.int32, (rows, 128), 1)
-    by_expert = jnp.zeros((rows, 128), jnp.float32)
-    for k in range(routes.shape[1]):
-        by_expert += jnp.where(routes[:, k : k + 1] == lanes, route_weights[:, k : k + 1], 0.0)
     route_rows = route_all.shape[1]
-    route_all[sp] = by_expert.T[:route_rows]
+    names = lax.broadcasted_iota(jnp.int32, (route_rows, rows), 0)
+    by_expert = jnp.zeros((route_rows, rows), jnp.float32)
+    for k in range(routes.shape[0]):
+        by_expert += jnp.where(routes[k : k + 1, :] == names, route_weights[k : k + 1, :], 0.0)
+    route_all[sp] = by_expert
 
     def route_copy(d):
         to = (sp + d) % n_sp
@@ -411,85 +414,89 @@
 
     tile = 32
 
-    def mix_rows(i, carry):
-        part = pl.ds(pl.multiple_of(i * tile, tile), tile)
-        value = mix_out[part, :]
-        scaled = value * lax.rsqrt(jnp.mean(value * value, axis=1, keepdims=True) + epsilon)
-        summed = (stream[part, :].astype(jnp.float32) + scaled * mix_norm[...]).astype(jnp.bfloat16)
-        mixed[part, :] = summed
-        wide = summed.astype(jnp.float32)
-        wide = wide * lax.rsqrt(jnp.mean(wide * wide, axis=1, keepdims=True) + epsilon)
-        tokens[sp, part, :] = (wide * ffn_norm[...]).astype(jnp.bfloat16)
-        return carry
-
-    lax.fori_loop(0, rows // tile, mix_rows, 0)
-
-    def piece(block, kind, whose):
-        start = whose * half_rows + (0 if kind == XF else first_rows)
-        count = first_rows if kind == XF else half_rows - first_rows
-        return tokens.at[block, pl.ds(pl.multiple_of(start, 16), count), :]
-
-    def ag_copy(block, kind, way):
+    def mix_rows(first, count):
+        def body(i, carry):
+            part = pl.ds(pl.multiple_of(first + i * tile, tile), tile)
+            value = mix_out[part, :]
+            scaled = value * lax.rsqrt(jnp.mean(value * value, axis=1, keepdims=True) + epsilon)
+            summed = stream[part, :].astype(jnp.float32) + scaled * mix_norm[...]
+            summed = summed.astype(jnp.bfloat16)
+            mixed[part, :] = summed
+            wide = summed.astype(jnp.float32)
+            wide = wide * lax.rsqrt(jnp.mean(wide * wide, axis=1, keepdims=True) + epsilon)
+            tokens[sp, part, :] = (wide * ffn_norm[...]).astype(jnp.bfloat16)
+            return carry
+
+        lax.fori_loop(0, count // tile, body, 0)
+
+    def piece(block, half, kind, whose):
+        first = pl.multiple_of(half * half_rows + whose * core_rows, 16)
+        span = pl.ds(0, first_cols) if kind == XF else pl.ds(first_cols, width - first_cols)
+        return tokens.at[block, pl.ds(first, core_rows), span]
+
+    def ag_copy(block, half, kind, way):
         to_sp = {UP: sp + x_size, DOWN: sp - x_size, ACROSS: z * x_size + (1 - x), SIBLING: sp}[way]
-        recv = ag_recv.at[block, kind + (2 if way == SIBLING else 0)]
-        ref = piece(block, kind, core)
+        recv = ag_recv.at[block, half, kind + (2 if way == SIBLING else 0)]
+        ref = piece(block, half, kind, core)
         return remote(
-            ref, ref, ag_send.at[block, kind, way], recv, to_sp, sibling if way == SIBLING else tp
-        )
-
-    def ag_arrived(block, kind, from_sibling):
+            ref,
+            ref,
+            ag_send.at[block, half, kind, way],
+            recv,
+            to_sp,
+            sibling if way == SIBLING else tp,
+        )
+
+    def ag_arrived(block, half, kind, from_sibling):
         whose = 1 - core if from_sibling else core
-        ref = piece(block, kind, whose)
-        recv = ag_recv.at[block, kind + (2 if from_sibling else 0)]
-        remote(ref, ref, ag_send.at[block, kind, SIBLING], recv, sp, sibling).wait_recv()
-
-    def ag_ways(zc, col_is_own, kind, act):
+        ref = piece(block, half, kind, whose)
+        recv = ag_recv.at[block, half, kind + (2 if from_sibling else 0)]
+        remote(ref, ref, ag_send.at[block, half, kind, SIBLING], recv, sp, sibling).wait_recv()
+
+    def ag_ways(zc, half, col_is_own, kind, act):
         block = zc * x_size + (x if col_is_own else 1 - x)
-        along = col_is_own or kind == XF
-
-        if along:
+
+        if col_is_own and kind == XF:
+
+            @pl.when(zc == z)
+            def _():
+                act(ag_copy(block, half, kind, ACROSS))
+
+        if col_is_own or kind == XF:
 
             @pl.when((zc <= z) & (z < far_z))
             def _():
-                act(ag_copy(block, kind, UP))
+                act(ag_copy(block, half, kind, UP))
 
             @pl.when((zc >= z) & (z > 0))
             def _():
-                act(ag_copy(block, kind, DOWN))
+                act(ag_copy(block, half, kind, DOWN))
 
         if col_is_own and kind == ZF:
-            act(ag_copy(block, kind, ACROSS))
-        if col_is_own and kind == XF:
-
-            @pl.when(zc == z)
-            def _():
-                act(ag_copy(block, kind, ACROSS))
-
+            act(ag_copy(block, half, kind, ACROSS))
         if col_is_own:
 
             @pl.when(zc != z)
             def _():
-                act(ag_copy(block, kind, SIBLING))
+                act(ag_copy(block, half, kind, SIBLING))
 
         else:
-            act(ag_copy(block, kind, SIBLING))
+            act(ag_copy(block, half, kind, SIBLING))
 
     def start(copy):
         copy.start()
 
-    def take(zc, col_is_own, kind):
+    def take(zc, half, col_is_own, kind):
         block = zc * x_size + (x if col_is_own else 1 - x)
-        ag_arrived(block, kind, False)
-        ag_ways(zc, col_is_own, kind, start)
-
-    def take_set(zc):
-        take(zc, True, ZF)
-        take(zc, True, XF)
-        take(zc, False, XF)
-        take(zc, False, ZF)
-
-    ag_ways(z, True, XF, start)
-    ag_ways(z, True, ZF, start)
+        ag_arrived(block, half, kind, False)
+        ag_ways(zc, half, col_is_own, kind, start)
+
+    for whose in range(core_count):
+        for half in range(halves):
+            mix_rows(half * half_rows + (core if whose == 0 else 1 - core) * core_rows, core_rows)
+            if whose == 0:
+                ag_ways(z, half, True, XF, start)
+                ag_ways(z, half, True, ZF, start)
 
     for d in range(1, n_sp):
         src_sp = (sp + d) % n_sp
@@ -506,47 +513,69 @@
         plane = jnp.where(step <= low_z, low_z - step, step)
         return jnp.where(upper, far_z - plane, plane)
 
+    inner = low_z > 0
+
+    def unit_at(k):
+        paired = inner & (k >= 2) & (k < 6)
+        step = jnp.where(paired, 1 + k % 2, k // halves)
+        return plane_at(step), jnp.where(paired, k // 4, k % halves)
+
     n_hidden = hidden.shape[1]
     hidden_tile = min(256, n_hidden)
 
-    def part_copy(block, q_y):
+    def span_of(half):
+        return pl.ds(pl.multiple_of(half * half_rows, half_rows), half_rows)
+
+    def part_copy(block, half, q_y):
         q = q_y * core_count + (1 - core)
         return remote(
-            parts.at[block, q],
-            parts_in.at[block, q_y],
-            part_send.at[block, q_y],
-            part_recv.at[block, q_y],
+            parts.at[block, q, span_of(half)],
+            parts_in.at[block, q_y, span_of(half)],
+            part_send.at[block, half, q_y],
+            part_recv.at[block, half, q_y],
             sp,
             sibling,
         )
 
-    def pair_copy(block):
+    def pair_copy(block, half):
         return remote(
-            pair_out.at[block], pair_in.at[block], pair_send.at[block], pair_recv.at[block], sp, opposite
-        )
-
-    def side_copy(zc):
+            pair_out.at[block, span_of(half)],
+            pair_in.at[block, span_of(half)],
+            pair_send.at[block, half],
+            pair_recv.at[block, half],
+            sp,
+            opposite,
+        )
+
+    def side_copy(zc, half):
         return remote(
-            side_out.at[zc],
-            side_in.at[zc],
-            side_send.at[zc],
-            side_recv.at[zc],
+            side_out.at[zc, span_of(half)],
+            side_in.at[zc, span_of(half)],
+            side_send.at[zc, half],
+            side_recv.at[zc, half],
             z * x_size + (1 - x),
             tp,
         )
 
-    def far_copy(zc):
+    def far_copy(zc, half):
         return remote(
-            far_out.at[zc], far_in.at[z], far_send.at[zc], far_recv.at[z], zc * x_size + x, tp
-        )
-
-    def compute(block):
-        own_row = lax.broadcasted_iota(jnp.int32, (route_rows, rows), 0) == sp
-        weight = jnp.sum(jnp.where(own_row, route_all[block], 0.0), axis=0, keepdims=True)
-        weight = jnp.broadcast_to(weight, (128, rows)).T
+            far_out.at[zc, span_of(half)],
+            far_in.at[z, span_of(half)],
+            far_send.at[zc, half],
+            far_recv.at[z, half],
+            zc * x_size + x,
+            tp,
+        )
+
+    def compute(block, half):
+        own_row = lax.broadcasted_iota(jnp.int32, (route_rows, half_rows), 0) == sp
+        weight = jnp.sum(
+            jnp.where(own_row, route_all[block, :, span_of(half)], 0.0), axis=0, keepdims=True
+        )
+        weight = jnp.broadcast_to(weight, (128, half_rows)).T
         for j in range(n_hidden // hidden_tile):
             span = slice(j * hidden_tile, (j + 1) * hidden_tile)
-            data = tokens[block]
+            data = tokens[block, span_of(half), :]
             gate = jnp.dot(data, w_gate[:, span], preferred_element_type=jnp.float32)
             up = jnp.dot(data, w_up[:, span], preferred_element_type=jnp.float32)
             gate_cut = jnp.minimum(gate + gate_bias[:, span], clamp_limit)
@@ -561,115 +590,131 @@
             whose = jnp.where(i < 2, 1 - core, core)
             q = (i % 2) * core_count + whose
             at = pl.ds(pl.multiple_of(q * cols, cols), cols)
-            parts[block, q] = jnp.dot(
+            parts[block, q, span_of(half), :] = jnp.dot(
                 hidden[...], w_down[:, at], preferred_element_type=jnp.float32
             ).astype(jnp.bfloat16)
 
             @pl.when(i < 2)
             def _():
-                part_copy(block, i % 2).start()
+                part_copy(block, half, i % 2).start()
 
             return carry
 
         lax.fori_loop(0, n_tp, down, 0)
 
-    def join_cores(block):
+    def wide_of(ref, *at):
+        return ref[at].astype(jnp.float32)
+
+    def join_cores(block, half):
+        at = span_of(half)
         for q_y in range(n_tp // core_count):
-            part_copy(block, q_y).wait_recv()
-        away = parts[block, opposite].astype(jnp.float32) + parts_in[block, 1 - y].astype(jnp.float32)
-        pair_out[block] = away.astype(jnp.bfloat16)
-        pair_copy(block).start()
-        pair_keep[block] = parts[block, tp].astype(jnp.float32) + parts_in[block, y].astype(
-            jnp.float32
-        )
-
-    def join_pair_other(step):
-        zc = plane_at(step)
+            part_copy(block, half, q_y).wait_recv()
+        away = wide_of(parts, block, opposite, at) + wide_of(parts_in, block, 1 - y, at)
+        pair_out[block, at, :] = away.astype(jnp.bfloat16)
+        pair_copy(block, half).start()
+        pair_keep[block, at, :] = wide_of(parts, block, tp, at) + wide_of(parts_in, block, y, at)
+
+    def join_pair_other(k):
+        zc, half = unit_at(k)
+        at = span_of(half)
         block = zc * x_size + (1 - x)
-        pair_copy(block).wait_recv()
-        side_out[zc] = (pair_keep[block] + pair_in[block].astype(jnp.float32)).astype(jnp.bfloat16)
-        side_copy(zc).start()
-
-    def join_pair_own(step):
-        zc = plane_at(step)
+        pair_copy(block, half).wait_recv()
+        both = pair_keep[block, at, :] + wide_of(pair_in, block, at)
+        side_out[zc, at, :] = both.astype(jnp.bfloat16)
+        side_copy(zc, half).start()
+
+    def join_pair_own(k):
+        zc, half = unit_at(k)
+        at = span_of(half)
         block = zc * x_size + x
-        pair_copy(block).wait_recv()
-        total[zc] = pair_keep[block] + pair_in[block].astype(jnp.float32)
-
-    def join_sides(step):
-        zc = plane_at(step)
-        side_copy(zc).wait_recv()
-        value = total[zc] + side_in[zc].astype(jnp.float32)
-        total[zc] = value
+        pair_copy(block, half).wait_recv()
+        total[zc, at, :] = pair_keep[block, at, :] + wide_of(pair_in, block, at)
+
+    def join_sides(k):
+        zc, half = unit_at(k)
+        at = span_of(half)
+        side_copy(zc, half).wait_recv()
+        value = total[zc, at, :] + wide_of(side_in, zc, at)
+        total[zc, at, :] = value
 
         @pl.when(zc != z)
         def _():
-            far_out[zc] = value.astype(jnp.bfloat16)
-            far_copy(zc).start()
-
-    def step_body(step, carry):
-        zc = plane_at(step)
-        inner = low_z > 0
-
-        @pl.when((step >= 1) & ((step != 2) | (low_z == 0)))
+            far_out[zc, at, :] = value.astype(jnp.bfloat16)
+            far_copy(zc, half).start()
+
+    units = nz * halves
+
+    def unit_body(k, carry):
+        zc, half = unit_at(k)
+        own, other = zc * x_size + x, zc * x_size + (1 - x)
+
+        @pl.when(inner & (k >= 1) & (k + 1 < units))
         def _():
-            take_set(zc)
-
-        if nz > 2:
-
-            @pl.when((step == 1) & inner)
-            def _():
-                take_set(plane_at(2))
-
-        col = jnp.where(step == 0, x, 1 - x)
-        first, second = zc * x_size + col, zc * x_size + (1 - col)
-
-        @pl.when(step >= 1)
+            z_next, half_next = unit_at(k + 1)
+            take(z_next, half_next, True, ZF)
+            take(z_next, half_next, True, XF)
+            take(z_next, half_next, False, XF)
+
+        @pl.when((~inner) & (k >= halves))
         def _():
-            ag_arrived(first, XF, True)
-            ag_arrived(first, ZF, True)
-
-        compute(first)
-        join_cores(first)
-
-        @pl.when(step == 0)
+            take(zc, half, True, ZF)
+            take(zc, half, True, XF)
+
+        @pl.when(k >= halves)
         def _():
-            take(z, False, XF)
-            take(z, False, ZF)
-
-        @pl.when(step >= 1)
+            ag_arrived(own, half, XF, True)
+            ag_arrived(own, half, ZF, True)
+
+        compute(own, half)
+        join_cores(own, half)
+
+        @pl.when((~inner) | (k < halves))
         def _():
-            join_pair_other(step - 1)
-            join_pair_own(step - 1)
-
-        @pl.when(step >= 2)
+            take(zc, half, False, XF)
+
+        @pl.when(k >= 1)
         def _():
-            join_sides(step - 2)
-
-        ag_arrived(second, XF, True)
-        ag_arrived(second, ZF, True)
-        compute(second)
-        join_cores(second)
+            join_pair_own(k - 1)
+            join_pair_other(k - 1)
+
+        @pl.when((~inner) & (k >= 2))
+        def _():
+            join_sides(k - 2)
+
+        take(zc, half, False, ZF)
+        ag_arrived(other, half, XF, True)
+        ag_arrived(other, half, ZF, True)
+        compute(other, half)
+        join_cores(other, half)
         return carry
 
-    lax.fori_loop(0, nz, step_body, 0)
-    join_pair_other(nz - 1)
-    if nz > 1:
-        join_sides(nz - 2)
-    join_pair_own(nz - 1)
-    join_sides(nz - 1)
+    lax.fori_loop(0, units, unit_body, 0)
+
+    @pl.when(inner)
+    def _():
+        def sides(k, carry):
+            join_sides(k)
+            return carry
+
+        lax.fori_loop(0, units - 2, sides, 0)
+
+    join_pair_own(units - 1)
+    join_pair_other(units - 1)
+    join_sides(units - 2)
+    join_sides(units - 1)
 
     combined = total[z]
     for d in range(1, nz):
         src_z = (z + d) % nz
-        remote(
-            far_out.at[src_z],
-            far_in.at[src_z],
-            far_send.at[src_z],
-            far_recv.at[src_z],
-            src_z * x_size + x,
-            tp,
-        ).wait_recv()
+        for half in range(halves):
+            remote(
+                far_out.at[src_z, span_of(half)],
+                far_in.at[src_z, span_of(half)],
+                far_send.at[src_z, half],
+                far_recv.at[src_z, half],
+                src_z * x_size + x,
+                tp,
+            ).wait_recv()
         combined += far_in[src_z].astype(jnp.float32)
     total[z] = combined
 
@@ -711,24 +756,25 @@
     for d in range(1, n_sp):
         sent(route_copy(d))
 
-    def all_sent(zc, carry):
+    def all_sent(k, carry):
+        zc, half = k // halves, k % halves
         for col_is_own in (True, False):
             for kind in (XF, ZF):
-                ag_ways(zc, col_is_own, kind, sent)
+                ag_ways(zc, half, col_is_own, kind, sent)
         for i in range(x_size):
             block = zc * x_size + i
             for q_y in range(n_tp // core_count):
-                sent(part_copy(block, q_y))
-            sent(pair_copy(block))
-        sent(side_copy(zc))
+                sent(part_copy(block, half, q_y))
+            sent(pair_copy(block, half))
+        sent(side_copy(zc, half))
 
         @pl.when(zc != z)
         def _():
-            sent(far_copy(zc))
+            sent(far_copy(zc, half))
 
         return carry
 
-    lax.fori_loop(0, nz, all_sent, 0)
+    lax.fori_loop(0, units, all_sent, 0)
 
 
 def gathered_shards(*args):
@@ -743,6 +789,7 @@
     bf16, f32 = jnp.bfloat16, jnp.float32
     row_args = (2, 3, 6, 7, 15)
     args = [a.reshape(1, -1) if i in row_args else a for i, a in enumerate(args)]
+    args[8], args[9] = args[8].T, args[9].T
     in_hbm = (4, 5, 10, 11, 14)
     in_specs = [
         pl.BlockSpec(memory_space=pl.ANY if i in in_hbm else pltpu.VMEM) for i in range(len(args))
@@ -766,7 +813,7 @@
         pltpu.VMEM((rows, width), f32),
         pltpu.VMEM((rows, width), bf16),
         pltpu.VMEM((n_sp, route_rows, rows), f32),
-        pltpu.VMEM((rows, n_hidden), bf16),
+        pltpu.VMEM((rows // halves, n_hidden), bf16),
         pltpu.VMEM((n_sp, n_tp, rows, cols), bf16),
         pltpu.VMEM((n_sp, n_tp // core_count, rows, cols), bf16),
         pltpu.VMEM((n_sp, rows, cols), bf16),
@@ -779,22 +826,22 @@
         pltpu.VMEM((nz, rows, cols), bf16),
         pltpu.VMEM((n_tp, 8, rows), f32),
         dma((5,)),
-        dma((n_sp, 2, 4)),
-        dma((n_sp, 4)),
+        dma((n_sp, halves, 2, 4)),
+        dma((n_sp, halves, 4)),
         dma((n_tp, 3)),
         dma((n_tp, 3)),
         dma((2, n_tp)),
         dma((n_tp, 2)),
         dma((n_sp,)),
         dma((n_sp,)),
-        dma((n_sp, n_tp // core_count)),
-        dma((n_sp, n_tp // core_count)),
-        dma((n_sp,)),
-        dma((n_sp,)),
-        dma((nz,)),
-        dma((nz,)),
-        dma((nz,)),
-        dma((nz,)),
+        dma((n_sp, halves, n_tp // core_count)),
+        dma((n_sp, halves, n_tp // core_count)),
+        dma((n_sp, halves)),
+        dma((n_sp, halves)),
+        dma((nz, halves)),
+        dma((nz, halves)),
+        dma((nz, halves)),
+        dma((nz, halves)),
         dma((n_tp,)),
         dma((n_tp,)),
     ]
@@ -823,8 +870,8 @@
         n_tp == 2 * core_count
         and n_sp % x_size == 0
         and w_gate.shape[0] == 1
-        and rows % 128 == 0
-        and rows // core_count > first_rows
+        and rows % (128 * halves) == 0
+        and width % (128 * first_share[0]) == 0
         and cols % 128 == 0
         and n_hidden % 256 == 0
         and pool_in.shape[1] == 128

time: 127 us -> 113 us (0.89)
  Pallas kernels: 122 us -> 111 us
  local copies, waits for them, and re-layouts: 4.63 us -> 1.67 us
    pallas_call x1, Pallas kernels: 122 us -> 111 us  [gathered_shards(): pl.pallas_call(functools.partial(layer_kernel, nz), out_shape=jax.ShapeDt...]
    unnamed x3 -> x1, local copies, waits for them, and re-layouts: 4.63 us -> 1.67 us
where the time goes in v2:
time: 113 us
  Pallas kernels  111 us (98%)
  local copies, waits for them, and re-layouts  1.67 us (1%)
    pallas_call x1, Pallas kernels, gathered_shards(): pl.pallas_call(functools.partial(layer_kernel, nz), out_shape=jax.ShapeDt...  111 us

profile of v2, /device:TPU:0, one launch (start us, length us, event | category | flops | bytes accessed | tf_op | source)
XLA Modules:
  0.0 112.6 jit_solution(14150171440866188009)
XLA Ops:
  0.0 110.9 %layer.1 = bf16[256,512]{1,0:T(8,128)(2,1)} custom-call(bf16[256,128]{1,0:T(8,128)(2,1)} %pool_in.1, bf16[1,128,128]{2,1,0:T(8,128)(2,1)} %pool_weight.1, f32[1,128]{1,0:T(1,128)} %bitcast.13, f32[1,512]{1,0:T(1,128)} %bitcast.11, bf16[512,2048]{1,0:T(8,128)(2,1)} %out_weight_hbm.1, bf16[256,2048]{1,0:T(8,128)(2,1)} %stream_hbm.1, f32[1,2048]{1,0:T(1,128)} %bitcast.7, ...), custom_call_target="tpu_custom_call" | custom-call | tf_op jit(solution)/shard_map/layer/pallas_call | solution.py:848
  110.9 1.7 %copy.18 = bf16[256,512]{1,0:T(8,128)(2,1)} copy(bf16[256,512]{1,0:T(8,128)(2,1)} %layer.1) | data formatting | bytes 524288

commit v3 on v2

--- a/solution.py
+++ b/solution.py
@@ -242,6 +242,9 @@
             device_id_type=MESH,
         )
 
+    def wait_bytes(ref, sem):
+        pltpu.make_async_copy(ref, ref, sem).wait()
+
     loads = [
         pltpu.make_async_copy(src, dst, load_sem.at[i])
         for i, (src, dst) in enumerate(
@@ -282,34 +285,30 @@
 
     edge = pool_edges.shape[2]
 
-    def edge_copy(side, to_tp, d):
+    def edge_copy(side, to_tp):
         src = pool_in.at[pl.ds(rows - edge, edge)] if side == 0 else pool_in.at[pl.ds(0, edge)]
         return remote(
             src,
             pool_edges.at[tp, side],
-            edge_send.at[side, d],
-            edge_recv.at[tp, side],
+            edge_send.at[side],
+            edge_recv.at[side],
             sp + 1 if side == 0 else sp - 1,
             to_tp,
         )
 
-    def edge_loop(side, act):
+    for side in range(2):
+
         @pl.when(sp < n_sp - 1 if side == 0 else sp > 0)
         def _():
             for d in range(n_tp):
-                act(edge_copy(side, (tp + d) % n_tp, d))
-
-    for side in range(2):
-        edge_loop(side, lambda copy: copy.start())
+                edge_copy(side, (tp + d) % n_tp).start()
 
     def front_copies(d):
         to = (tp + d) % n_tp
         return [
-            remote(pool_in, pool_all.at[tp], front_send.at[d, 0], front_recv.at[tp, 0], sp, to),
-            remote(
-                pool_weight.at[0], weight_all.at[tp], front_send.at[d, 1], front_recv.at[tp, 1], sp, to
-            ),
-            remote(pool_scale, scale_all.at[tp], front_send.at[d, 2], front_recv.at[tp, 2], sp, to),
+            remote(pool_in, pool_all.at[tp], front_send.at[0], front_recv.at[0], sp, to),
+            remote(pool_weight.at[0], weight_all.at[tp], front_send.at[1], front_recv.at[1], sp, to),
+            remote(pool_scale, scale_all.at[tp], front_send.at[2], front_recv.at[2], sp, to),
         ]
 
     for d in range(1, n_tp):
@@ -329,36 +328,21 @@
     def route_copy(d):
         to = (sp + d) % n_sp
         return remote(
-            route_all.at[sp], route_all.at[sp], route_send.at[d], route_recv.at[sp], to, tp
+            route_all.at[sp], route_all.at[sp], route_send.at[0], route_recv.at[0], to, tp
         )
 
     for d in range(1, n_sp):
         route_copy(d).start()
 
-    for d in range(1, n_tp):
-        src_tp = (tp + d) % n_tp
-        for i, (src, dst) in enumerate(
-            (
-                (pool_in, pool_all),
-                (pool_weight.at[0], weight_all),
-                (pool_scale, scale_all),
-            )
-        ):
-            remote(
-                src, dst.at[src_tp], front_send.at[d, i], front_recv.at[src_tp, i], sp, src_tp
-            ).wait_recv()
+    others = pl.ds(0, n_tp - 1)
+    front_all = (pool_all, weight_all, scale_all)
+    for i, ref in enumerate(front_all):
+        wait_bytes(ref.at[others], front_recv.at[i])
 
     @pl.when(sp > 0)
     def _():
+        wait_bytes(pool_edges.at[:, 0], edge_recv.at[0])
         for g in range(n_tp):
-            remote(
-                pool_in.at[pl.ds(0, edge)],
-                pool_edges.at[g, 0],
-                edge_send.at[0, 0],
-                edge_recv.at[g, 0],
-                sp - 1,
-                tp,
-            ).wait_recv()
             padded[g, 0:reach_rows, :] = pool_edges[g, 0].astype(jnp.float32)[edge - reach_rows :]
 
     @pl.when(sp == 0)
@@ -367,15 +351,8 @@
 
     @pl.when(sp < n_sp - 1)
     def _():
+        wait_bytes(pool_edges.at[:, 1], edge_recv.at[1])
         for g in range(n_tp):
-            remote(
-                pool_in.at[pl.ds(0, edge)],
-                pool_edges.at[g, 1],
-                edge_send.at[0, 0],
-                edge_recv.at[g, 1],
-                sp + 1,
-                tp,
-            ).wait_recv()
             padded[g, reach_rows + rows :, :] = pool_edges[g, 1].astype(jnp.float32)[:reach_rows]
 
     @pl.when(sp == n_sp - 1)
@@ -434,75 +411,90 @@
         span = pl.ds(0, first_cols) if kind == XF else pl.ds(first_cols, width - first_cols)
         return tokens.at[block, pl.ds(first, core_rows), span]
 
-    def ag_copy(block, half, kind, way):
+    def ag_copy(block, half, kind, way, lane_of=0):
         to_sp = {UP: sp + x_size, DOWN: sp - x_size, ACROSS: z * x_size + (1 - x), SIBLING: sp}[way]
-        recv = ag_recv.at[block, half, kind + (2 if way == SIBLING else 0)]
+        recv = ag_recv.at[block, half, 2 if way == SIBLING else kind]
         ref = piece(block, half, kind, core)
-        return remote(
-            ref,
-            ref,
-            ag_send.at[block, half, kind, way],
-            recv,
-            to_sp,
-            sibling if way == SIBLING else tp,
-        )
-
-    def ag_arrived(block, half, kind, from_sibling):
-        whose = 1 - core if from_sibling else core
-        ref = piece(block, half, kind, whose)
-        recv = ag_recv.at[block, half, kind + (2 if from_sibling else 0)]
-        remote(ref, ref, ag_send.at[block, half, kind, SIBLING], recv, sp, sibling).wait_recv()
-
-    def ag_ways(zc, half, col_is_own, kind, act):
+        to_tp = sibling if way == SIBLING else tp
+        return remote(ref, ref, ag_send.at[way, lane_of], recv, to_sp, to_tp)
+
+    def ag_arrived(block, half, kind):
+        wait_bytes(piece(block, half, kind, core), ag_recv.at[block, half, kind])
+
+    def sibling_arrived(block, half):
+        first = pl.multiple_of(half * half_rows + (1 - core) * core_rows, 16)
+        wait_bytes(tokens.at[block, pl.ds(first, core_rows), :], ag_recv.at[block, half, 2])
+
+    def ag_start(zc, half, col_is_own, kind):
         block = zc * x_size + (x if col_is_own else 1 - x)
 
         if col_is_own and kind == XF:
 
             @pl.when(zc == z)
             def _():
-                act(ag_copy(block, half, kind, ACROSS))
-
+                ag_copy(block, half, kind, ACROSS).start()
+
+        lane_of = 0 if col_is_own else 1
         if col_is_own or kind == XF:
 
             @pl.when((zc <= z) & (z < far_z))
             def _():
-                act(ag_copy(block, half, kind, UP))
+                ag_copy(block, half, kind, UP, lane_of).start()
 
             @pl.when((zc >= z) & (z > 0))
             def _():
-                act(ag_copy(block, half, kind, DOWN))
+                ag_copy(block, half, kind, DOWN, lane_of).start()
 
         if col_is_own and kind == ZF:
-            act(ag_copy(block, half, kind, ACROSS))
-        if col_is_own:
+
+            @pl.when(zc == z)
+            def _():
+                ag_copy(block, half, kind, ACROSS).start()
 
             @pl.when(zc != z)
             def _():
-                act(ag_copy(block, half, kind, SIBLING))
+                ag_copy(block, half, kind, ACROSS, 1).start()
+
+        if col_is_own:
+
+            @pl.when(zc != z)
+            def _():
+                ag_copy(block, half, kind, SIBLING).start()
 
         else:
-            act(ag_copy(block, half, kind, SIBLING))
-
-    def start(copy):
-        copy.start()
+            ag_copy(block, half, kind, SIBLING).start()
+
+    def ag_sent():
+        carried = pl.ds(0, halves * core_rows)
+        xf, zf = pl.ds(0, first_cols), pl.ds(first_cols, width - first_cols)
+        wait_bytes(tokens.at[pl.ds(0, n_sp - 1), carried, :], ag_send.at[SIBLING, 0])
+        wait_bytes(tokens.at[0, carried, :], ag_send.at[ACROSS, 0])
+        if nz > 1:
+            wait_bytes(tokens.at[pl.ds(0, nz - 1), carried, zf], ag_send.at[ACROSS, 1])
+        for at_z in range(nz):
+
+            @pl.when(z == at_z)
+            def _():
+                if at_z < far_z:
+                    wait_bytes(tokens.at[pl.ds(0, at_z + 1), carried, :], ag_send.at[UP, 0])
+                    wait_bytes(tokens.at[pl.ds(0, at_z + 1), carried, xf], ag_send.at[UP, 1])
+                if at_z > 0:
+                    wait_bytes(tokens.at[pl.ds(0, nz - at_z), carried, :], ag_send.at[DOWN, 0])
+                    wait_bytes(tokens.at[pl.ds(0, nz - at_z), carried, xf], ag_send.at[DOWN, 1])
 
     def take(zc, half, col_is_own, kind):
         block = zc * x_size + (x if col_is_own else 1 - x)
-        ag_arrived(block, half, kind, False)
-        ag_ways(zc, half, col_is_own, kind, start)
+        ag_arrived(block, half, kind)
+        ag_start(zc, half, col_is_own, kind)
 
     for whose in range(core_count):
         for half in range(halves):
             mix_rows(half * half_rows + (core if whose == 0 else 1 - core) * core_rows, core_rows)
             if whose == 0:
-                ag_ways(z, half, True, XF, start)
-                ag_ways(z, half, True, ZF, start)
-
-    for d in range(1, n_sp):
-        src_sp = (sp + d) % n_sp
-        remote(
-            route_all.at[sp], route_all.at[src_sp], route_send.at[d], route_recv.at[src_sp], src_sp, tp
-        ).wait_recv()
+                ag_start(z, half, True, XF)
+                ag_start(z, half, True, ZF)
+
+    wait_bytes(route_all.at[pl.ds(0, n_sp - 1)], route_recv.at[0])
     for load in loads[2:]:
         load.wait()
 
@@ -531,8 +523,8 @@
         return remote(
             parts.at[block, q, span_of(half)],
             parts_in.at[block, q_y, span_of(half)],
-            part_send.at[block, half, q_y],
-            part_recv.at[block, half, q_y],
+            part_send.at[0],
+            part_recv.at[block, half],
             sp,
             sibling,
         )
@@ -541,7 +533,7 @@
         return remote(
             pair_out.at[block, span_of(half)],
             pair_in.at[block, span_of(half)],
-            pair_send.at[block, half],
+            pair_send.at[0],
             pair_recv.at[block, half],
             sp,
             opposite,
@@ -551,7 +543,7 @@
         return remote(
             side_out.at[zc, span_of(half)],
             side_in.at[zc, span_of(half)],
-            side_send.at[zc, half],
+            side_send.at[0],
             side_recv.at[zc, half],
             z * x_size + (1 - x),
             tp,
@@ -561,8 +553,8 @@
         return remote(
             far_out.at[zc, span_of(half)],
             far_in.at[z, span_of(half)],
-            far_send.at[zc, half],
-            far_recv.at[z, half],
+            far_send.at[0],
+            far_recv.at[0],
             zc * x_size + x,
             tp,
         )
@@ -607,12 +599,19 @@
 
     def join_cores(block, half):
         at = span_of(half)
-        for q_y in range(n_tp // core_count):
-            part_copy(block, half, q_y).wait_recv()
+        wait_bytes(parts_in.at[block, :, at], part_recv.at[block, half])
         away = wide_of(parts, block, opposite, at) + wide_of(parts_in, block, 1 - y, at)
         pair_out[block, at, :] = away.astype(jnp.bfloat16)
         pair_copy(block, half).start()
         pair_keep[block, at, :] = wide_of(parts, block, tp, at) + wide_of(parts_in, block, y, at)
+
+    def join_own_cores(k):
+        zc, half = unit_at(k)
+        join_cores(zc * x_size + x, half)
+
+    def join_other_cores(k):
+        zc, half = unit_at(k)
+        join_cores(zc * x_size + (1 - x), half)
 
     def join_pair_other(k):
         zc, half = unit_at(k)
@@ -644,78 +643,144 @@
 
     units = nz * halves
 
+    def take_first(k):
+        z_next, half_next = unit_at(k)
+        take(z_next, half_next, True, ZF)
+
+    def take_ahead(k):
+        z_next, half_next = unit_at(k)
+        take(z_next, half_next, True, ZF)
+        take(z_next, half_next, True, XF)
+        take(z_next, half_next, False, XF)
+
+    def compute_own(k):
+        zc, half = unit_at(k)
+        block = zc * x_size + x
+
+        @pl.when(k >= halves)
+        def _():
+            sibling_arrived(block, half)
+
+        compute(block, half)
+
+    def compute_other(k):
+        zc, half = unit_at(k)
+        block = zc * x_size + (1 - x)
+        sibling_arrived(block, half)
+        compute(block, half)
+
+    def take_other(k):
+        zc, half = unit_at(k)
+        take(zc, half, False, ZF)
+
+    for k in range(halves):
+        compute_own(k)
+        if k == 0:
+            take(z, 0, False, XF)
+    take_other(0)
+    join_own_cores(0)
+    compute_other(0)
+    join_own_cores(1)
+    take(z, 1, False, XF)
+    if units > halves:
+
+        @pl.when(~inner)
+        def _():
+            take_first(2)
+
+    join_other_cores(0)
+    take_other(1)
+    join_pair_own(0)
+    if units > halves:
+
+        @pl.when(inner)
+        def _():
+            take_ahead(2)
+            take_ahead(3)
+
+    def sides(k, carry):
+        join_sides(k)
+        return carry
+
     def unit_body(k, carry):
         zc, half = unit_at(k)
-        own, other = zc * x_size + x, zc * x_size + (1 - x)
-
-        @pl.when(inner & (k >= 1) & (k + 1 < units))
-        def _():
-            z_next, half_next = unit_at(k + 1)
-            take(z_next, half_next, True, ZF)
-            take(z_next, half_next, True, XF)
-            take(z_next, half_next, False, XF)
-
-        @pl.when((~inner) & (k >= halves))
-        def _():
-            take(zc, half, True, ZF)
+
+        @pl.when(~inner)
+        def _():
             take(zc, half, True, XF)
 
-        @pl.when(k >= halves)
-        def _():
-            ag_arrived(own, half, XF, True)
-            ag_arrived(own, half, ZF, True)
-
-        compute(own, half)
-        join_cores(own, half)
-
-        @pl.when((~inner) | (k < halves))
+        compute_other(k - 1)
+
+        @pl.when((~inner) & (k + 1 < units))
+        def _():
+            take_first(k + 1)
+
+        compute_own(k)
+
+        @pl.when(~inner)
         def _():
             take(zc, half, False, XF)
 
-        @pl.when(k >= 1)
-        def _():
-            join_pair_own(k - 1)
-            join_pair_other(k - 1)
-
-        @pl.when((~inner) & (k >= 2))
-        def _():
-            join_sides(k - 2)
-
-        take(zc, half, False, ZF)
-        ag_arrived(other, half, XF, True)
-        ag_arrived(other, half, ZF, True)
-        compute(other, half)
-        join_cores(other, half)
+        @pl.when(inner & (k == 2))
+        def _():
+            take_ahead(4)
+            take_ahead(5)
+
+        @pl.when(inner & ((k == 3) | (k >= 5)))
+        def _():
+            ahead = jnp.where(k == 3, 6, k + 2)
+
+            @pl.when(ahead < units)
+            def _():
+                take_ahead(ahead)
+
+        take_other(k)
+        join_other_cores(k - 1)
+        join_own_cores(k)
+        join_pair_own(k - 1)
+        join_pair_other(k - 2)
+
+        @pl.when(((~inner) & (k >= 3)) | (inner & (k >= 7)))
+        def _():
+            join_sides(k - 3)
+
+        @pl.when(inner & (k == 6))
+        def _():
+            lax.fori_loop(0, 4, sides, 0)
+
         return carry
 
-    lax.fori_loop(0, units, unit_body, 0)
-
-    @pl.when(inner)
-    def _():
-        def sides(k, carry):
-            join_sides(k)
-            return carry
-
-        lax.fori_loop(0, units - 2, sides, 0)
+    lax.fori_loop(halves, units, unit_body, 0)
+    compute_other(units - 1)
+    join_other_cores(units - 1)
+    join_pair_other(units - 2)
 
     join_pair_own(units - 1)
+    if units > 2:
+        join_sides(units - 3)
     join_pair_other(units - 1)
     join_sides(units - 2)
     join_sides(units - 1)
 
+    for side in range(2):
+
+        @pl.when(sp < n_sp - 1 if side == 0 else sp > 0)
+        def _():
+            wait_bytes(pool_edges.at[:, side], edge_send.at[side])
+
+    for i, ref in enumerate(front_all):
+        wait_bytes(ref.at[others], front_send.at[i])
+    wait_bytes(route_all.at[pl.ds(0, n_sp - 1)], route_send.at[0])
+    ag_sent()
+    wait_bytes(parts_in, part_send.at[0])
+    wait_bytes(pair_out, pair_send.at[0])
+    wait_bytes(side_out, side_send.at[0])
+
     combined = total[z]
+    if nz > 1:
+        wait_bytes(far_in.at[pl.ds(0, nz - 1)], far_recv.at[0])
     for d in range(1, nz):
-        src_z = (z + d) % nz
-        for half in range(halves):
-            remote(
-                far_out.at[src_z, span_of(half)],
-                far_in.at[src_z, span_of(half)],
-                far_send.at[src_z, half],
-                far_recv.at[src_z, half],
-                src_z * x_size + x,
-                tp,
-            ).wait_recv()
-        combined += far_in[src_z].astype(jnp.float32)
+        combined += far_in[(z + d) % nz].astype(jnp.float32)
     total[z] = combined
 
     own_squares = jnp.sum(combined * combined, axis=1, keepdims=True)
@@ -723,18 +788,15 @@
 
     def squares_copy(d):
         return remote(
-            squares.at[tp], squares.at[tp], sq_send.at[d], sq_recv.at[tp], sp, (tp + d) % n_tp
+            squares.at[tp], squares.at[tp], sq_send.at[0], sq_recv.at[0], sp, (tp + d) % n_tp
         )
 
     for d in range(1, n_tp):
         squares_copy(d).start()
-    summed = squares[tp]
-    for d in range(1, n_tp):
-        src_tp = (tp + d) % n_tp
-        remote(
-            squares.at[tp], squares.at[src_tp], sq_send.at[d], sq_recv.at[src_tp], sp, src_tp
-        ).wait_recv()
-        summed += squares[src_tp]
+    wait_bytes(squares.at[others], sq_recv.at[0])
+    summed = squares[0]
+    for i in range(1, n_tp):
+        summed += squares[i]
     row_scale = lax.rsqrt(summed[:1] / width + epsilon)
     row_scale = jnp.broadcast_to(row_scale, (128, rows)).T
     for i in range(cols // 128):
@@ -744,37 +806,9 @@
             jnp.bfloat16
         )
 
-    def sent(copy):
-        copy.wait_send()
-
-    for side in range(2):
-        edge_loop(side, sent)
-    for d in range(1, n_tp):
-        for copy in front_copies(d):
-            sent(copy)
-        sent(squares_copy(d))
-    for d in range(1, n_sp):
-        sent(route_copy(d))
-
-    def all_sent(k, carry):
-        zc, half = k // halves, k % halves
-        for col_is_own in (True, False):
-            for kind in (XF, ZF):
-                ag_ways(zc, half, col_is_own, kind, sent)
-        for i in range(x_size):
-            block = zc * x_size + i
-            for q_y in range(n_tp // core_count):
-                sent(part_copy(block, half, q_y))
-            sent(pair_copy(block, half))
-        sent(side_copy(zc, half))
-
-        @pl.when(zc != z)
-        def _():
-            sent(far_copy(zc, half))
-
-        return carry
-
-    lax.fori_loop(0, units, all_sent, 0)
+    wait_bytes(squares.at[others], sq_send.at[0])
+    if nz > 1:
+        wait_bytes(far_out.at[pl.ds(0, nz - 1)], far_send.at[0])
 
 
 def gathered_shards(*args):
@@ -826,24 +860,24 @@
         pltpu.VMEM((nz, rows, cols), bf16),
         pltpu.VMEM((n_tp, 8, rows), f32),
         dma((5,)),
-        dma((n_sp, halves, 2, 4)),
-        dma((n_sp, halves, 4)),
-        dma((n_tp, 3)),
-        dma((n_tp, 3)),
-        dma((2, n_tp)),
-        dma((n_tp, 2)),
-        dma((n_sp,)),
-        dma((n_sp,)),
-        dma((n_sp, halves, n_tp // core_count)),
-        dma((n_sp, halves, n_tp // core_count)),
+        dma((4, 2)),
+        dma((n_sp, halves, 3)),
+        dma((3,)),
+        dma((3,)),
+        dma((2,)),
+        dma((2,)),
+        dma((1,)),
+        dma((1,)),
+        dma((1,)),
         dma((n_sp, halves)),
+        dma((1,)),
         dma((n_sp, halves)),
+        dma((1,)),
         dma((nz, halves)),
-        dma((nz, halves)),
-        dma((nz, halves)),
-        dma((nz, halves)),
-        dma((n_tp,)),
-        dma((n_tp,)),
+        dma((1,)),
+        dma((1,)),
+        dma((1,)),
+        dma((1,)),
     ]
     return pl.pallas_call(
         functools.partial(layer_kernel, nz),

time: 113 us -> 98.6 us (0.87)
  Pallas kernels: 111 us -> 96.7 us
    pallas_call x1, Pallas kernels: 111 us -> 96.7 us  [gathered_shards(): pl.pallas_call(functools.partial(layer_kernel, nz), out_shape=jax.ShapeDt...]
where the time goes in v3:
time: 98.6 us; the launch traced here: 98.4 us
  Pallas kernels  96.7 us (98%)
  local copies, waits for them, and re-layouts  1.67 us (2%)
    pallas_call x1, Pallas kernels, gathered_shards(): pl.pallas_call(functools.partial(layer_kernel, nz), out_shape=jax.ShapeDt...  96.7 us

profile of v3, /device:TPU:0, one launch (start us, length us, event | category | flops | bytes accessed | tf_op | source)
XLA Modules:
  0.0 98.4 jit_solution(18351088571699975734)
XLA Ops:
  0.0 96.7 %layer.1 = bf16[256,512]{1,0:T(8,128)(2,1)} custom-call(bf16[256,128]{1,0:T(8,128)(2,1)} %pool_in.1, bf16[1,128,128]{2,1,0:T(8,128)(2,1)} %pool_weight.1, f32[1,128]{1,0:T(1,128)} %bitcast.13, f32[1,512]{1,0:T(1,128)} %bitcast.11, bf16[512,2048]{1,0:T(8,128)(2,1)} %out_weight_hbm.1, bf16[256,2048]{1,0:T(8,128)(2,1)} %stream_hbm.1, f32[1,2048]{1,0:T(1,128)} %bitcast.7, ...), custom_call_target="tpu_custom_call" | custom-call | tf_op jit(solution)/shard_map/layer/pallas_call | solution.py:882
  96.7 1.7 %copy.18 = bf16[256,512]{1,0:T(8,128)(2,1)} copy(bf16[256,512]{1,0:T(8,128)(2,1)} %layer.1) | data formatting | bytes 524288

commit v4 on v3

--- a/solution.py
+++ b/solution.py
@@ -145,7 +145,8 @@
 x_size = 2
 core_count = 2
 halves = 2
-first_share = 8, 3
+subs = 2
+first_share = 16, 5
 vmem_limit = 60 * 1024 * 1024
 UP, DOWN, ACROSS, SIBLING = range(4)
 XF, ZF = range(2)
@@ -451,7 +452,7 @@
             def _():
                 ag_copy(block, half, kind, ACROSS).start()
 
-            @pl.when(zc != z)
+            @pl.when((zc != z) & ~from_end(zc))
             def _():
                 ag_copy(block, half, kind, ACROSS, 1).start()
 
@@ -463,18 +464,39 @@
 
         else:
             ag_copy(block, half, kind, SIBLING).start()
+
+        if not col_is_own and kind == ZF and nz > 2:
+
+            @pl.when((zc == z) & (z == 0))
+            def _():
+                ag_copy(block, half, kind, UP, 2).start()
+
+            @pl.when((zc == z) & (z == far_z))
+            def _():
+                ag_copy(block, half, kind, DOWN, 2).start()
+
+    def from_end(zc):
+        at_end = ((zc == 0) & (z == 1)) | ((zc == far_z) & (z == far_z - 1))
+        return at_end & (z > 0) & (z < far_z)
 
     def ag_sent():
         carried = pl.ds(0, halves * core_rows)
         xf, zf = pl.ds(0, first_cols), pl.ds(first_cols, width - first_cols)
         wait_bytes(tokens.at[pl.ds(0, n_sp - 1), carried, :], ag_send.at[SIBLING, 0])
         wait_bytes(tokens.at[0, carried, :], ag_send.at[ACROSS, 0])
-        if nz > 1:
-            wait_bytes(tokens.at[pl.ds(0, nz - 1), carried, zf], ag_send.at[ACROSS, 1])
         for at_z in range(nz):
 
             @pl.when(z == at_z)
             def _():
+                across = nz - 1
+                if 0 < at_z < far_z:
+                    across -= (at_z == 1) + (at_z == far_z - 1)
+                if across > 0:
+                    wait_bytes(tokens.at[pl.ds(0, across), carried, zf], ag_send.at[ACROSS, 1])
+                if nz > 2 and at_z == 0:
+                    wait_bytes(tokens.at[0, carried, zf], ag_send.at[UP, 2])
+                if nz > 2 and at_z == far_z:
+                    wait_bytes(tokens.at[0, carried, zf], ag_send.at[DOWN, 2])
                 if at_z < far_z:
                     wait_bytes(tokens.at[pl.ds(0, at_z + 1), carried, :], ag_send.at[UP, 0])
                     wait_bytes(tokens.at[pl.ds(0, at_z + 1), carried, xf], ag_send.at[UP, 1])
@@ -507,10 +529,16 @@
 
     inner = low_z > 0
 
+    inner_order = {2: (1, 0), 3: (2, 0), 4: (1, 1), 5: (2, 1)}
+    if nz > 3:
+        inner_order.update({5: (3, 0), 6: (3, 1), 7: (2, 1)})
+
     def unit_at(k):
-        paired = inner & (k >= 2) & (k < 6)
-        step = jnp.where(paired, 1 + k % 2, k // halves)
-        return plane_at(step), jnp.where(paired, k // 4, k % halves)
+        step, half = k // halves, k % halves
+        for at, (inner_step, inner_half) in inner_order.items():
+            step = jnp.where(inner & (k == at), inner_step, step)
+            half = jnp.where(inner & (k == at), inner_half, half)
+        return plane_at(step), half
 
     n_hidden = hidden.shape[1]
     hidden_tile = min(256, n_hidden)
@@ -529,30 +557,38 @@
             sibling,
         )
 
-    def pair_copy(block, half):
+    sub_rows = half_rows // subs
+
+    def sub_of(half, sub):
+        return pl.ds(pl.multiple_of(half * half_rows + sub * sub_rows, sub_rows), sub_rows)
+
+    def pair_copy(block, half, sub):
+        at = sub_of(half, sub)
         return remote(
-            pair_out.at[block, span_of(half)],
-            pair_in.at[block, span_of(half)],
+            pair_out.at[block, at],
+            pair_in.at[block, at],
             pair_send.at[0],
-            pair_recv.at[block, half],
+            pair_recv.at[block, half, sub],
             sp,
             opposite,
         )
 
-    def side_copy(zc, half):
+    def side_copy(zc, half, sub):
+        at = sub_of(half, sub)
         return remote(
-            side_out.at[zc, span_of(half)],
-            side_in.at[zc, span_of(half)],
+            side_out.at[zc, at],
+            side_in.at[zc, at],
             side_send.at[0],
-            side_recv.at[zc, half],
+            side_recv.at[zc, half, sub],
             z * x_size + (1 - x),
             tp,
         )
 
-    def far_copy(zc, half):
+    def far_copy(zc, half, sub):
+        at = sub_of(half, sub)
         return remote(
-            far_out.at[zc, span_of(half)],
-            far_in.at[z, span_of(half)],
+            far_out.at[zc, at],
+            far_in.at[z, at],
             far_send.at[0],
             far_recv.at[0],
             zc * x_size + x,
@@ -598,11 +634,13 @@
         return ref[at].astype(jnp.float32)
 
     def join_cores(block, half):
+        wait_bytes(parts_in.at[block, :, span_of(half)], part_recv.at[block, half])
+        for sub in range(subs):
+            at = sub_of(half, sub)
+            away = wide_of(parts, block, opposite, at) + wide_of(parts_in, block, 1 - y, at)
+            pair_out[block, at, :] = away.astype(jnp.bfloat16)
+            pair_copy(block, half, sub).start()
         at = span_of(half)
-        wait_bytes(parts_in.at[block, :, at], part_recv.at[block, half])
-        away = wide_of(parts, block, opposite, at) + wide_of(parts_in, block, 1 - y, at)
-        pair_out[block, at, :] = away.astype(jnp.bfloat16)
-        pair_copy(block, half).start()
         pair_keep[block, at, :] = wide_of(parts, block, tp, at) + wide_of(parts_in, block, y, at)
 
     def join_own_cores(k):
@@ -615,31 +653,37 @@
 
     def join_pair_other(k):
         zc, half = unit_at(k)
-        at = span_of(half)
         block = zc * x_size + (1 - x)
-        pair_copy(block, half).wait_recv()
-        both = pair_keep[block, at, :] + wide_of(pair_in, block, at)
-        side_out[zc, at, :] = both.astype(jnp.bfloat16)
-        side_copy(zc, half).start()
+        for sub in range(subs):
+            at = sub_of(half, sub)
+            pair_copy(block, half, sub).wait_recv()
+            both = pair_keep[block, at, :] + wide_of(pair_in, block, at)
+            side_out[zc, at, :] = both.astype(jnp.bfloat16)
+            side_copy(zc, half, sub).start()
 
     def join_pair_own(k):
         zc, half = unit_at(k)
+        block = zc * x_size + x
+        for sub in range(subs):
+            pair_copy(block, half, sub).wait_recv()
         at = span_of(half)
-        block = zc * x_size + x
-        pair_copy(block, half).wait_recv()
         total[zc, at, :] = pair_keep[block, at, :] + wide_of(pair_in, block, at)
 
     def join_sides(k):
         zc, half = unit_at(k)
-        at = span_of(half)
-        side_copy(zc, half).wait_recv()
-        value = total[zc, at, :] + wide_of(side_in, zc, at)
-        total[zc, at, :] = value
-
-        @pl.when(zc != z)
-        def _():
-            far_out[zc, at, :] = value.astype(jnp.bfloat16)
-            far_copy(zc, half).start()
+        for sub in range(subs):
+            at = sub_of(half, sub)
+            side_copy(zc, half, sub).wait_recv()
+            value = total[zc, at, :] + wide_of(side_in, zc, at)
+
+            @pl.when(zc != z)
+            def _():
+                far_out[zc, at, :] = value.astype(jnp.bfloat16)
+                far_copy(zc, half, sub).start()
+
+            @pl.when(zc == z)
+            def _():
+                total[zc, at, :] = value
 
     units = nz * halves
 
@@ -647,11 +691,14 @@
         z_next, half_next = unit_at(k)
         take(z_next, half_next, True, ZF)
 
-    def take_ahead(k):
+    def take_rest(k):
         z_next, half_next = unit_at(k)
-        take(z_next, half_next, True, ZF)
         take(z_next, half_next, True, XF)
         take(z_next, half_next, False, XF)
+
+    def take_ahead(k):
+        take_first(k)
+        take_rest(k)
 
     def compute_own(k):
         zc, half = unit_at(k)
@@ -673,30 +720,25 @@
         zc, half = unit_at(k)
         take(zc, half, False, ZF)
 
-    for k in range(halves):
-        compute_own(k)
-        if k == 0:
-            take(z, 0, False, XF)
+    compute_own(0)
+    take(z, 0, False, XF)
+    compute_own(1)
+    join_own_cores(0)
     take_other(0)
-    join_own_cores(0)
+    join_own_cores(1)
     compute_other(0)
-    join_own_cores(1)
     take(z, 1, False, XF)
     if units > halves:
 
-        @pl.when(~inner)
-        def _():
-            take_first(2)
+        take_first(2)
+
+        @pl.when(inner)
+        def _():
+            take_first(3)
 
     join_other_cores(0)
     take_other(1)
     join_pair_own(0)
-    if units > halves:
-
-        @pl.when(inner)
-        def _():
-            take_ahead(2)
-            take_ahead(3)
 
     def sides(k, carry):
         join_sides(k)
@@ -711,53 +753,78 @@
 
         compute_other(k - 1)
 
-        @pl.when((~inner) & (k + 1 < units))
+        @pl.when((~inner) & (k <= 3) & (k + 1 < units))
         def _():
             take_first(k + 1)
 
+        @pl.when(inner & (k == 2))
+        def _():
+            take_rest(2)
+            take_rest(3)
+
         compute_own(k)
+        join_other_cores(k - 1)
 
         @pl.when(~inner)
         def _():
             take(zc, half, False, XF)
 
-        @pl.when(inner & (k == 2))
-        def _():
-            take_ahead(4)
-            take_ahead(5)
-
-        @pl.when(inner & ((k == 3) | (k >= 5)))
-        def _():
-            ahead = jnp.where(k == 3, 6, k + 2)
-
-            @pl.when(ahead < units)
-            def _():
-                take_ahead(ahead)
+        for at, ahead in ((2, (4, 7)), (3, (5,)), (4, (6,))) if nz > 3 else ((2, (4, 5)),):
+
+            @pl.when(inner & (k == at))
+            def _():
+                for unit in ahead:
+                    take_ahead(unit)
+
+        if units > 8:
+
+            @pl.when(inner & (k >= 6) & (k + 2 < units))
+            def _():
+                take_ahead(k + 2)
 
         take_other(k)
-        join_other_cores(k - 1)
         join_own_cores(k)
-        join_pair_own(k - 1)
+
+        @pl.when((~inner) & (k > 3) & (k + 1 < units))
+        def _():
+            take_first(k + 1)
+
         join_pair_other(k - 2)
 
-        @pl.when(((~inner) & (k >= 3)) | (inner & (k >= 7)))
+        @pl.when(k < units - 1)
+        def _():
+            join_pair_own(k - 1)
+
+        @pl.when((~inner) & (k >= 3))
         def _():
             join_sides(k - 3)
 
-        @pl.when(inner & (k == 6))
-        def _():
-            lax.fori_loop(0, 4, sides, 0)
+        @pl.when(inner & (k >= 6))
+        def _():
+            join_sides(k - 4)
+
+        @pl.when(inner & (k >= 6) & (k == units - 1))
+        def _():
+            join_sides(k - 3)
 
         return carry
 
     lax.fori_loop(halves, units, unit_body, 0)
     compute_other(units - 1)
     join_other_cores(units - 1)
+    if units > halves:
+        join_pair_own(units - 2)
     join_pair_other(units - 2)
 
+    @pl.when(inner)
+    def _():
+        lax.fori_loop(0, halves, sides, 0)
+        if units <= 6:
+            lax.fori_loop(max(units - 4, halves), units - 3, sides, 0)
+
+    if units > halves:
+        join_sides(units - 3)
     join_pair_own(units - 1)
-    if units > 2:
-        join_sides(units - 3)
     join_pair_other(units - 1)
     join_sides(units - 2)
     join_sides(units - 1)
@@ -860,7 +927,7 @@
         pltpu.VMEM((nz, rows, cols), bf16),
         pltpu.VMEM((n_tp, 8, rows), f32),
         dma((5,)),
-        dma((4, 2)),
+        dma((4, 3)),
         dma((n_sp, halves, 3)),
         dma((3,)),
         dma((3,)),
@@ -871,9 +938,9 @@
         dma((1,)),
         dma((n_sp, halves)),
         dma((1,)),
-        dma((n_sp, halves)),
+        dma((n_sp, halves, subs)),
         dma((1,)),
-        dma((nz, halves)),
+        dma((nz, halves, subs)),
         dma((1,)),
         dma((1,)),
         dma((1,)),

time: 98.6 us -> 93.1 us (0.944); the launches traced: 98.4 us -> 91.4 us
  Pallas kernels: 96.7 us -> 89.7 us
    pallas_call x1, Pallas kernels: 96.7 us -> 89.7 us  [gathered_shards(): pl.pallas_call(functools.partial(layer_kernel, nz), out_shape=jax.ShapeDt...]
where the time goes in v4:
time: 93.1 us; the launch traced here: 91.4 us
  Pallas kernels  89.7 us (96%)
  local copies, waits for them, and re-layouts  1.67 us (2%)
    pallas_call x1, Pallas kernels, gathered_shards(): pl.pallas_call(functools.partial(layer_kernel, nz), out_shape=jax.ShapeDt...  89.7 us

profile of v4, /device:TPU:0, one launch (start us, length us, event | category | flops | bytes accessed | tf_op | source)
XLA Modules:
  0.0 91.4 jit_solution(646367098350678084)
XLA Ops:
  0.0 89.7 %layer.1 = bf16[256,512]{1,0:T(8,128)(2,1)} custom-call(bf16[256,128]{1,0:T(8,128)(2,1)} %pool_in.1, bf16[1,128,128]{2,1,0:T(8,128)(2,1)} %pool_weight.1, f32[1,128]{1,0:T(1,128)} %bitcast.13, f32[1,512]{1,0:T(1,128)} %bitcast.11, bf16[512,2048]{1,0:T(8,128)(2,1)} %out_weight_hbm.1, bf16[256,2048]{1,0:T(8,128)(2,1)} %stream_hbm.1, f32[1,2048]{1,0:T(1,128)} %bitcast.7, ...), custom_call_target="tpu_custom_call" | custom-call | tf_op jit(solution)/shard_map/layer/pallas_call | solution.py:949
  89.7 1.7 %copy.18 = bf16[256,512]{1,0:T(8,128)(2,1)} copy(bf16[256,512]{1,0:T(8,128)(2,1)} %layer.1) | data formatting | bytes 524288

commit v5 on v4

--- a/solution.py
+++ b/solution.py
@@ -197,6 +197,7 @@
     total,
     far_out,
     far_in,
+    mid_in,
     squares,
     load_sem,
     ag_send,
@@ -215,6 +216,7 @@
     side_recv,
     far_send,
     far_recv,
+    mid_recv,
     sq_send,
     sq_recv,
 ):
@@ -595,6 +597,24 @@
             tp,
         )
 
+    end = (z == 0) | (z == far_z)
+
+    def goes_by_mid(from_z, to_z):
+        from_end_z = (from_z == 0) | (from_z == far_z)
+        return from_end_z & ((from_z - to_z == 2) | (to_z - from_z == 2))
+
+    def mid_copy(zc, half, sub):
+        at = sub_of(half, sub)
+        side = jnp.where(z == 0, 0, 1)
+        return remote(
+            far_out.at[zc, at],
+            mid_in.at[side, at],
+            far_send.at[0],
+            mid_recv.at[side, half, sub],
+            jnp.where(z == 0, 1, far_z - 1) * x_size + x,
+            tp,
+        )
+
     def compute(block, half):
         own_row = lax.broadcasted_iota(jnp.int32, (route_rows, half_rows), 0) == sp
         weight = jnp.sum(
@@ -674,16 +694,25 @@
         for sub in range(subs):
             at = sub_of(half, sub)
             side_copy(zc, half, sub).wait_recv()
-            value = total[zc, at, :] + wide_of(side_in, zc, at)
+            total[zc, at, :] += wide_of(side_in, zc, at)
+            for side, end_z in enumerate((0, far_z)):
+
+                @pl.when((~end) & goes_by_mid(end_z, zc) & (2 * z == zc + end_z))
+                def _():
+                    wait_bytes(mid_in.at[side, at], mid_recv.at[side, half, sub])
+                    total[zc, at, :] += wide_of(mid_in, side, at)
 
             @pl.when(zc != z)
             def _():
-                far_out[zc, at, :] = value.astype(jnp.bfloat16)
+                far_out[zc, at, :] = total[zc, at, :].astype(jnp.bfloat16)
+
+            @pl.when((zc != z) & goes_by_mid(z, zc))
+            def _():
+                mid_copy(zc, half, sub).start()
+
+            @pl.when((zc != z) & ~goes_by_mid(z, zc))
+            def _():
                 far_copy(zc, half, sub).start()
-
-            @pl.when(zc == z)
-            def _():
-                total[zc, at, :] = value
 
     units = nz * halves
 
@@ -799,7 +828,7 @@
         def _():
             join_sides(k - 3)
 
-        @pl.when(inner & (k >= 6))
+        @pl.when(inner & (k >= 6) & (k != 7))
         def _():
             join_sides(k - 4)
 
@@ -824,6 +853,13 @@
 
     if units > halves:
         join_sides(units - 3)
+
+        if units > 7:
+
+            @pl.when(inner)
+            def _():
+                join_sides(3)
+
     join_pair_own(units - 1)
     join_pair_other(units - 1)
     join_sides(units - 2)
@@ -843,12 +879,21 @@
     wait_bytes(pair_out, pair_send.at[0])
     wait_bytes(side_out, side_send.at[0])
 
+    for at_z in range(nz):
+        direct = [
+            i
+            for i in range(nz)
+            if i != at_z and not (i in (0, far_z) and abs(i - at_z) == 2)
+        ]
+
+        @pl.when(z == at_z)
+        def _():
+            if direct:
+                wait_bytes(far_in.at[pl.ds(0, len(direct))], far_recv.at[0])
+            for i in direct:
+                total[at_z] += far_in[i].astype(jnp.float32)
+
     combined = total[z]
-    if nz > 1:
-        wait_bytes(far_in.at[pl.ds(0, nz - 1)], far_recv.at[0])
-    for d in range(1, nz):
-        combined += far_in[(z + d) % nz].astype(jnp.float32)
-    total[z] = combined
 
     own_squares = jnp.sum(combined * combined, axis=1, keepdims=True)
     squares[tp] = jnp.broadcast_to(own_squares, (rows, 128)).T[:8]
@@ -925,6 +970,7 @@
         pltpu.VMEM((nz, rows, cols), f32),
         pltpu.VMEM((nz, rows, cols), bf16),
         pltpu.VMEM((nz, rows, cols), bf16),
+        pltpu.VMEM((2, rows, cols), bf16),
         pltpu.VMEM((n_tp, 8, rows), f32),
         dma((5,)),
         dma((4, 3)),
@@ -943,6 +989,7 @@
         dma((nz, halves, subs)),
         dma((1,)),
         dma((1,)),
+        dma((2, halves, subs)),
         dma((1,)),
         dma((1,)),
     ]

time: 93.1 us -> 91.5 us (0.983); the launches traced: 91.4 us -> 90.9 us
  no operation moved by 1% of the time
where the time goes in v5:
time: 91.5 us; the launch traced here: 90.9 us
  Pallas kernels  89.2 us (97%)
  local copies, waits for them, and re-layouts  1.67 us (2%)
    pallas_call x1, Pallas kernels, gathered_shards(): pl.pallas_call(functools.partial(layer_kernel, nz), out_shape=jax.ShapeDt...  89.2 us

profile of v5, /device:TPU:0, one launch (start us, length us, event | category | flops | bytes accessed | tf_op | source)
XLA Modules:
  0.0 90.9 jit_solution(12706984785051410835)
XLA Ops:
  0.0 89.2 %layer.1 = bf16[256,512]{1,0:T(8,128)(2,1)} custom-call(bf16[256,128]{1,0:T(8,128)(2,1)} %pool_in.1, bf16[1,128,128]{2,1,0:T(8,128)(2,1)} %pool_weight.1, f32[1,128]{1,0:T(1,128)} %bitcast.13, f32[1,512]{1,0:T(1,128)} %bitcast.11, bf16[512,2048]{1,0:T(8,128)(2,1)} %out_weight_hbm.1, bf16[256,2048]{1,0:T(8,128)(2,1)} %stream_hbm.1, f32[1,2048]{1,0:T(1,128)} %bitcast.7, ...), custom_call_target="tpu_custom_call" | custom-call | tf_op jit(solution)/shard_map/layer/pallas_call | solution.py:996
  89.2 1.7 %copy.18 = bf16[256,512]{1,0:T(8,128)(2,1)} copy(bf16[256,512]{1,0:T(8,128)(2,1)} %layer.1) | data formatting | bytes 524288

commit v6 on v5

--- a/solution.py
+++ b/solution.py
@@ -299,6 +299,19 @@
             to_tp,
         )
 
+    third = (1 - y) * core_count + (1 - core)
+    front_all = (pool_all, weight_all, scale_all)
+    front_own = (pool_in, pool_weight.at[0], pool_scale)
+
+    def front_copy(i, src, owner, source, to_tp):
+        return remote(
+            src, front_all[i].at[owner], front_send.at[i], front_recv.at[i, source], sp, to_tp
+        )
+
+    for i, src in enumerate(front_own):
+        front_copy(i, src, tp, 0, opposite).start()
+    for i, src in enumerate(front_own):
+        front_copy(i, src, tp, 1, sibling).start()
     for side in range(2):
 
         @pl.when(sp < n_sp - 1 if side == 0 else sp > 0)
@@ -306,17 +319,6 @@
             for d in range(n_tp):
                 edge_copy(side, (tp + d) % n_tp).start()
 
-    def front_copies(d):
-        to = (tp + d) % n_tp
-        return [
-            remote(pool_in, pool_all.at[tp], front_send.at[0], front_recv.at[0], sp, to),
-            remote(pool_weight.at[0], weight_all.at[tp], front_send.at[1], front_recv.at[1], sp, to),
-            remote(pool_scale, scale_all.at[tp], front_send.at[2], front_recv.at[2], sp, to),
-        ]
-
-    for d in range(1, n_tp):
-        for copy in front_copies(d):
-            copy.start()
     pool_all[tp] = pool_in[...]
     weight_all[tp] = pool_weight[0]
     scale_all[tp] = pool_scale[...]
@@ -338,9 +340,12 @@
         route_copy(d).start()
 
     others = pl.ds(0, n_tp - 1)
-    front_all = (pool_all, weight_all, scale_all)
     for i, ref in enumerate(front_all):
-        wait_bytes(ref.at[others], front_recv.at[i])
+        wait_bytes(ref.at[opposite], front_recv.at[i, 0])
+        front_copy(i, ref.at[opposite], opposite, 2, sibling).start()
+    for i, ref in enumerate(front_all):
+        wait_bytes(ref.at[sibling], front_recv.at[i, 1])
+        wait_bytes(ref.at[third], front_recv.at[i, 2])
 
     @pl.when(sp > 0)
     def _():
@@ -976,7 +981,7 @@
         dma((4, 3)),
         dma((n_sp, halves, 3)),
         dma((3,)),
-        dma((3,)),
+        dma((3, 3)),
         dma((2,)),
         dma((2,)),
         dma((1,)),

time: 91.5 us -> 91 us (level)
  no operation moved by 1% of the time
where the time goes in v6:
time: 91 us; the launch traced here: 90.8 us
  Pallas kernels  89.2 us (98%)
  local copies, waits for them, and re-layouts  1.67 us (2%)
    pallas_call x1, Pallas kernels, gathered_shards(): pl.pallas_call(functools.partial(layer_kernel, nz), out_shape=jax.ShapeDt...  89.2 us

profile of v6, /device:TPU:0, one launch (start us, length us, event | category | flops | bytes accessed | tf_op | source)
XLA Modules:
  0.0 90.8 jit_solution(11382127951269034088)
XLA Ops:
  0.0 89.2 %layer.1 = bf16[256,512]{1,0:T(8,128)(2,1)} custom-call(bf16[256,128]{1,0:T(8,128)(2,1)} %pool_in.1, bf16[1,128,128]{2,1,0:T(8,128)(2,1)} %pool_weight.1, f32[1,128]{1,0:T(1,128)} %bitcast.13, f32[1,512]{1,0:T(1,128)} %bitcast.11, bf16[512,2048]{1,0:T(8,128)(2,1)} %out_weight_hbm.1, bf16[256,2048]{1,0:T(8,128)(2,1)} %stream_hbm.1, f32[1,2048]{1,0:T(1,128)} %bitcast.7, ...), custom_call_target="tpu_custom_call" | custom-call | tf_op jit(solution)/shard_map/layer/pallas_call | solution.py:1001
  89.2 1.7 %copy.18 = bf16[256,512]{1,0:T(8,128)(2,1)} copy(bf16[256,512]{1,0:T(8,128)(2,1)} %layer.1) | data formatting | bytes 524288
